TPU v7x, 32 devices: a whole 2x2x4 slice. The times are simulated.
32 devices in a mesh: sp: 8 (over z, y), tp: 4 (over x, core).
Axes of the slice: x: 2, y: 2, z: 4, core: 2. Of those that a mesh axis runs over, the one named last changes fastest.
Arguments:
- latent: bfloat16 [2048, 2048], P('sp'), may hold values from -6 to 6
- context: bfloat16 [512, 2048], P('sp'), may hold values from -6 to 6
- condition: float32 [2048], P('sp'), may hold values from -6 to 6
- ctx_condition: float32 [2048], P('sp'), may hold values from -6 to 6
- shift_weight: bfloat16 [2048, 2048], P('sp', 'tp'), may hold values from -0.125 to 0.125
- scale_weight: bfloat16 [2048, 2048], P('sp', 'tp'), may hold values from -0.125 to 0.125
- gate_weight: bfloat16 [2048, 2048], P('sp', 'tp'), may hold values from -0.125 to 0.125
- norm_gain: float32 [2048], replicated, may hold values from 0.1 to 1.9
- query_weight: bfloat16 [2048, 1024], P(None, 'tp'), may hold values from -0.125 to 0.125
- key_weight: bfloat16 [2048, 1024], P(None, 'tp'), may hold values from -0.125 to 0.125
- value_weight: bfloat16 [2048, 1024], P(None, 'tp'), may hold values from -0.125 to 0.125
- query_gain: float32 [64], replicated, may hold values from 0.6 to 6.5
- key_gain: float32 [64], replicated, may hold values from 0.6 to 6.5
- offset_bias: float32 [16, 15, 31], P('tp'), may hold values from 1 to 3
- out_weight: bfloat16 [1024, 2048], P('tp'), may hold values from -0.75 to 0.75
Outputs:
- mixed_rows: bfloat16 [2048, 2048], P('sp')
All inputs are finite; a program needn't handle non-finite values.
Results may differ from a plain program's by a relative error of at most 0.01405.
The roundings to bfloat16 on the way count: a program that leaves them out, or rounds other values in their place, can miss the bound.
Values may be sent and summed in bfloat16 or wider, within the bound.
A program may use at most 64 MiB of HBM per device.

v0:
```python
import functools

import jax
import jax.numpy as jnp
from jax import lax
from jax.experimental import pallas as pl
from jax.experimental.pallas import tpu as pltpu
from jax.sharding import PartitionSpec as P

HEAD_DIM = 64
GRID_W = 64
WIN_ROWS = 8
WIN_COLS = 16


EPS = 1e-06


def extended(x, sides, width):
    for axis, dim in sides:
        count, length = (lax.axis_size(axis), x.shape[dim])
        up = [(i, (i + 1) % count) for i in range(count - 1)]
        down = [(j, i) for i, j in up]
        last = lax.slice_in_dim(x, length - width, length, axis=dim)
        initial = lax.slice_in_dim(x, 0, width, axis=dim)
        before = lax.ppermute(last, axis, up)
        after = lax.ppermute(initial, axis, down)
        x = jnp.concatenate([before, x, after], axis=dim)
    return x


def modulate(rows_in, norm_gain, shift_vec, scale_vec):
    values = rows_in.astype(jnp.float32)
    normed = values * lax.rsqrt(jnp.mean(values * values, axis=-1, keepdims=True) + EPS)
    return (normed * norm_gain * (1.0 + scale_vec) + shift_vec).astype(jnp.bfloat16)


def head_norm(projected, head_gain):
    row_count = projected.shape[0]
    split_heads = projected.reshape(row_count, -1, head_gain.shape[0])
    normed = split_heads * lax.rsqrt(
        jnp.mean(split_heads * split_heads, axis=-1, keepdims=True) + EPS
    )
    return (normed * head_gain).astype(jnp.bfloat16).reshape(row_count, -1)


def per_device_plain(
    latent,
    context,
    condition,
    ctx_condition,
    shift_weight,
    scale_weight,
    gate_weight,
    norm_gain,
    query_weight,
    key_weight,
    value_weight,
    query_gain,
    key_gain,
    offset_bias,
    out_weight,
):
    activations = jax.nn.silu(jnp.stack([condition, ctx_condition])).astype(jnp.bfloat16)
    part_shift = jnp.dot(activations, shift_weight, preferred_element_type=jnp.float32)
    part_scale = jnp.dot(activations, scale_weight, preferred_element_type=jnp.float32)
    part_gate = jnp.dot(activations[:1], gate_weight, preferred_element_type=jnp.float32)
    block_cols = shift_weight.shape[1]
    first_col = lax.axis_index("tp") * block_cols

    def spread(piece_part):
        padded_vec = jnp.zeros((piece_part.shape[0], block_cols * lax.axis_size("tp")), jnp.float32)
        return lax.dynamic_update_slice_in_dim(padded_vec, piece_part, first_col, 1)

    shift_vec, scale_vec, gate_vec = lax.psum(
        (spread(part_shift), spread(part_scale), spread(part_gate)), ("sp", "tp")
    )
    hidden = modulate(latent, norm_gain, shift_vec[0], scale_vec[0])
    queries = head_norm(
        jnp.dot(hidden, query_weight, preferred_element_type=jnp.float32), query_gain
    )
    keys_lat = head_norm(jnp.dot(hidden, key_weight, preferred_element_type=jnp.float32), key_gain)
    values_lat = jnp.dot(hidden, value_weight, preferred_element_type=jnp.float32).astype(
        jnp.bfloat16
    )
    ctx_hidden = modulate(
        lax.all_gather(context, "sp", axis=0, tiled=True), norm_gain, shift_vec[1], scale_vec[1]
    )
    ctx_keys = head_norm(
        jnp.dot(ctx_hidden, key_weight, preferred_element_type=jnp.float32), key_gain
    )
    ctx_values = jnp.dot(ctx_hidden, value_weight, preferred_element_type=jnp.float32).astype(
        jnp.bfloat16
    )
    ctx_pairs = jnp.concatenate([ctx_keys, ctx_values], axis=1)
    col_width = keys_lat.shape[1]
    heads_dev = col_width // HEAD_DIM
    local_rows = keys_lat.shape[0] // GRID_W
    halo_rows = WIN_ROWS // 2
    window_keys = WIN_ROWS * GRID_W
    key_value = jnp.concatenate([keys_lat, values_lat], axis=1).reshape(
        local_rows, GRID_W, 2 * col_width
    )
    padded = extended(key_value, (("sp", 0),), halo_rows)
    first_row = lax.axis_index("sp") * local_rows
    total_rows = local_rows * lax.axis_size("sp")
    global_rows = first_row + jnp.arange(local_rows, dtype=jnp.int32)
    band_start = jnp.clip(global_rows - halo_rows, 0, total_rows - WIN_ROWS)
    band_global = band_start[:, None] + jnp.arange(WIN_ROWS, dtype=jnp.int32)[None, :]
    banded = jnp.take(padded, band_global - first_row + halo_rows, axis=0)
    key_band = banded[..., :col_width].reshape(local_rows, window_keys, heads_dev, HEAD_DIM)
    value_band = banded[..., col_width:].reshape(local_rows, window_keys, heads_dev, HEAD_DIM)
    row_steps = band_global - global_rows[:, None] + WIN_ROWS - 1
    row_hot = (
        row_steps[:, :, None] == jnp.arange(2 * WIN_ROWS - 1, dtype=jnp.int32)[None, None, :]
    ).astype(jnp.float32)
    column_ids = jnp.arange(GRID_W, dtype=jnp.int32)
    col_steps = (
        jnp.clip(column_ids[None, :] - column_ids[:, None], 1 - WIN_COLS, WIN_COLS - 1)
        + WIN_COLS
        - 1
    )
    col_hot = (
        col_steps[:, :, None] == jnp.arange(2 * WIN_COLS - 1, dtype=jnp.int32)[None, None, :]
    ).astype(jnp.float32)
    col_start = jnp.clip(column_ids - WIN_COLS // 2, 0, GRID_W - WIN_COLS)
    col_open = (column_ids[None, :] >= col_start[:, None]) & (
        column_ids[None, :] < col_start[:, None] + WIN_COLS
    )
    col_table = jnp.einsum("hab,qkb->haqk", offset_bias, col_hot, precision=lax.Precision.HIGHEST)
    col_table = jnp.where(col_open[None, None, :, :], col_table, -jnp.inf)
    offset_terms = jnp.einsum(
        "rja,haqk->hrqjk",
        row_hot,
        jnp.where(col_open[None, None], col_table, 0.0),
        precision=lax.Precision.HIGHEST,
    )
    offset_terms = jnp.where(col_open[None, None, :, None, :], offset_terms, -jnp.inf)
    offset_terms = offset_terms.reshape(heads_dev, local_rows, GRID_W, window_keys)
    score_scale = HEAD_DIM ** (-0.5)
    q_grid = queries.reshape(local_rows, GRID_W, heads_dev, HEAD_DIM)
    scores = (
        jnp.einsum("rqhd,rnhd->hrqn", q_grid, key_band, preferred_element_type=jnp.float32)
        * score_scale
        + offset_terms
    )
    ctx_count = ctx_pairs.shape[0]
    ctx_keys_all = ctx_pairs[:, :col_width].reshape(ctx_count, heads_dev, HEAD_DIM)
    ctx_values_all = ctx_pairs[:, col_width:].reshape(ctx_count, heads_dev, HEAD_DIM)
    ctx_scores = (
        jnp.einsum("rqhd,nhd->hrqn", q_grid, ctx_keys_all, preferred_element_type=jnp.float32)
        * score_scale
    )
    row_max = jnp.maximum(jnp.max(scores, axis=3), jnp.max(ctx_scores, axis=3))
    local_exp = jnp.exp(scores - row_max[..., None])
    ctx_exp = jnp.exp(ctx_scores - row_max[..., None])
    denominator = jnp.sum(local_exp, axis=3) + jnp.sum(ctx_exp, axis=3)
    local_weights = (local_exp / denominator[..., None]).astype(jnp.bfloat16)
    ctx_weights = (ctx_exp / denominator[..., None]).astype(jnp.bfloat16)
    combined = jnp.einsum(
        "hrqn,rnhd->rqhd", local_weights, value_band, preferred_element_type=jnp.float32
    ) + jnp.einsum(
        "hrqn,nhd->rqhd", ctx_weights, ctx_values_all, preferred_element_type=jnp.float32
    )
    attended = combined.astype(jnp.bfloat16).reshape(local_rows * GRID_W, col_width)
    partial_value = jnp.dot(attended, out_weight, preferred_element_type=jnp.float32)
    branch = lax.psum(partial_value.astype(jnp.bfloat16), "tp").astype(jnp.float32)
    return (latent.astype(jnp.float32) + gate_vec[0] * branch).astype(jnp.bfloat16)


MESH = pl.DeviceIdType.MESH
MASKED = -1e30
F32 = jnp.float32
BF16 = jnp.bfloat16


def fused_kernel(
    n_sp,
    n_tp,
    latent,
    context,
    shift_w,
    scale_w,
    gate_w,
    query_w,
    key_w,
    value_w,
    out_w,
    cond,
    ctx_cond,
    norm_gain,
    query_gain,
    key_gain,
    bias_in,
    out,
    x_in,
    x_norm,
    hid,
    w_mod,
    w_qkv,
    w_out,
    mod_sp,
    mod_tp,
    q_stage,
    k_stage,
    v_stage,
    ck_stage,
    cv_stage,
    q_all,
    k_all,
    v_all,
    ctx_k,
    ctx_v,
    bias_pad,
    bias_lines,
    table,
    att_slab,
    att,
    local_sem,
    mod_send,
    mod_recv,
    modt_send,
    modt_recv,
    pair_send,
    pair_recv,
    halo_send,
    halo_recv,
    ctx_send,
    ctx_recv,
    wo_send,
    wo_recv,
    att_send,
    att_recv,
):
    me_s, me_t = lax.axis_index("sp"), lax.axis_index("tp")
    rows, d = latent.shape
    c_rows = context.shape[0]
    width = key_w.shape[1]
    heads = width // HEAD_DIM
    block = shift_w.shape[1]
    l_rows = rows // GRID_W
    halo = WIN_ROWS // 2
    win = WIN_ROWS * GRID_W
    core = lax.rem(me_t, 2)
    chip = lax.div(me_t, 2)
    partner = me_t + 1 - 2 * core
    n_x = n_tp // 2
    side = lax.rem(me_s, 2)
    slab = lax.div(me_s, 2)
    mate = me_s + 1 - 2 * side
    last_slab = n_sp // 2 - 1
    half = width // 2
    half_heads = heads // 2

    def remote(src, dst, send, recv, s, t):
        return pltpu.make_async_remote_copy(
            src_ref=src, dst_ref=dst, send_sem=send, recv_sem=recv,
            device_id=(s, t), device_id_type=MESH,
        )

    barrier = pltpu.get_barrier_semaphore()
    for k in range(1, n_sp):
        pl.semaphore_signal(
            barrier, inc=1, device_id=(lax.rem(me_s + k, n_sp), me_t), device_id_type=MESH
        )
    for k in range(1, n_tp):
        pl.semaphore_signal(
            barrier, inc=1, device_id=(me_s, lax.rem(me_t + k, n_tp)), device_id_type=MESH
        )

    loads = [
        (shift_w, w_mod.at[0]),
        (scale_w, w_mod.at[1]),
        (gate_w, w_mod.at[2]),
        (context, x_in.at[pl.ds(0, c_rows)]),
        (latent, x_in.at[pl.ds(c_rows, rows)]),
        (key_w, w_qkv.at[0]),
        (value_w, w_qkv.at[1]),
        (query_w, w_qkv.at[2]),
        (out_w, w_out.at[me_t]),
    ]
    copies = [pltpu.make_async_copy(a, b, local_sem.at[i]) for i, (a, b) in enumerate(loads)]
    for c in copies[:3]:
        c.start()

    def silu(v):
        return v / (1.0 + jnp.exp(-v))

    two = (16, cond.shape[1])
    row_id = lax.broadcasted_iota(jnp.int32, two, 0)
    act0 = jnp.broadcast_to(silu(cond[...]), two)
    act1 = jnp.broadcast_to(silu(ctx_cond[...]), two)

    def placed(first, second):
        picked = jnp.where(row_id == first, act0, 0.0)
        if second is not None:
            picked = jnp.where(row_id == second, act1, picked)
        return picked.astype(BF16)

    part = jnp.zeros((16, block), F32)
    for i, (first, second) in enumerate(((0, 1), (2, 3), (4, None))):
        copies[i].wait()
        part += jnp.dot(placed(first, second), w_mod[i], preferred_element_type=F32)
    for c in copies[3:]:
        c.start()
    mod_sp[me_s] = part[:8]
    pl.semaphore_wait(barrier, n_sp + n_tp - 2)
    sends = []
    for k in range(1, n_sp):
        peer = lax.rem(me_s + k, n_sp)
        c = remote(
            mod_sp.at[me_s], mod_sp.at[me_s], mod_send.at[k], mod_recv.at[me_s], peer, me_t
        )
        c.start()
        sends.append(c)

    def gather_start(view, sems, source=None):
        send, recv = sems
        mine = view(me_t) if source is None else source
        started = [remote(mine, view(me_t), send(0), recv(me_t), me_s, partner)]
        for k in range(1, n_x):
            far = 2 * lax.rem(chip + k, n_x) + core
            started.append(remote(mine, view(me_t), send(k), recv(me_t), me_s, far))
        for c in reversed(started):
            c.start()
        sends.extend(started)

    def gather_forward(view, sems):
        send, recv = sems
        for k in range(1, n_x):
            came = 2 * lax.rem(chip + n_x - k, n_x) + core
            c = remote(view(came), view(came), send(n_x + k), recv(came), me_s, partner)
            c.wait_recv()
            c.start()
            sends.append(c)

    def gather_finish(view, sems):
        send, recv = sems
        remote(
            view(partner), view(partner), send(0), recv(partner), me_s, partner
        ).wait_recv()
        for k in range(1, n_x):
            came = 2 * lax.rem(chip + n_x - k, n_x) + 1 - core
            remote(
                view(came), view(came), send(n_x + k), recv(came), me_s, partner
            ).wait_recv()

    early = width // 4
    wo_rows = (pl.ds(0, early), pl.ds(early, width - early))

    def wo_view(c):
        return lambda j: w_out.at[j, wo_rows[c]]

    def wo_source(c):
        return out_w.at[wo_rows[c]]

    def wo_sems(c):
        return (lambda k: wo_send.at[c, k]), (lambda k: wo_recv.at[c, k])

    def att_view(h):
        return lambda j: att.at[j, h]

    def att_sems(n):
        return (lambda k: att_send.at[n, k]), (lambda k: att_recv.at[n, k])

    gather_start(wo_view(0), wo_sems(0), wo_source(0))

    copies[3].wait()
    copies[4].wait()
    step = 32

    def norm_rows(i, carry):
        at = pl.ds(pl.multiple_of(i * step, step), step)
        v = x_in[at, :].astype(F32)
        r = lax.rsqrt(jnp.mean(v * v, axis=-1, keepdims=True) + EPS)
        x_norm[at, :] = v * r * norm_gain[...]
        return carry

    lax.fori_loop(0, (rows + c_rows) // step, norm_rows, 0)

    pair = 2 * GRID_W
    q_col = lax.broadcasted_iota(jnp.int32, (GRID_W, pair), 0)
    k_col = lax.broadcasted_iota(jnp.int32, (GRID_W, pair), 1) % GRID_W
    col0 = jnp.clip(q_col - WIN_COLS // 2, 0, GRID_W - WIN_COLS)
    col_open = (k_col >= col0) & (k_col < col0 + WIN_COLS)
    n_pairs = 2 * WIN_ROWS - 2
    bias_pad[...] = jnp.zeros_like(bias_pad)
    for h in range(heads):
        bias_pad[h, : 2 * WIN_ROWS - 1, : 2 * WIN_COLS - 1] = bias_in[:, h, :]
    for h in range(half_heads):
        head = side * half_heads + h
        upper = pltpu.roll(bias_pad[head, 1 : n_pairs + 1, :], GRID_W, 1)
        bias_lines[h, :n_pairs, :] = bias_pad[head, :n_pairs, :] + upper
        for a in range(n_pairs):
            line = jnp.broadcast_to(bias_lines[h, a : a + 1, :], (GRID_W, pair))
            rolled = pltpu.roll(line, pair - (WIN_COLS - 1), 1, stride=1, stride_axis=0)
            table[a, h * GRID_W : (h + 1) * GRID_W, :] = jnp.where(col_open, rolled, MASKED)

    for k in range(1, n_sp):
        peer = lax.rem(me_s + k, n_sp)
        remote(
            mod_sp.at[peer], mod_sp.at[peer], mod_send.at[k], mod_recv.at[peer], peer, me_t
        ).wait_recv()
    total = mod_sp[0]
    for k in range(1, n_sp):
        total = total + mod_sp[k]
    mod_tp[me_t] = total
    for k in range(1, n_tp):
        peer = lax.rem(me_t + k, n_tp)
        c = remote(
            mod_tp.at[me_t], mod_tp.at[me_t], modt_send.at[k], modt_recv.at[me_t], me_s, peer
        )
        c.start()
        sends.append(c)

    gather_start(wo_view(1), wo_sems(1), wo_source(1))

    for k in range(1, n_tp):
        peer = lax.rem(me_t + k, n_tp)
        remote(
            mod_tp.at[peer], mod_tp.at[peer], modt_send.at[k], modt_recv.at[peer], me_s, peer
        ).wait_recv()

    def vec(r):
        return jnp.concatenate([mod_tp[j][r : r + 1, :] for j in range(n_tp)], axis=1)

    def modulate_rows(first, count, shift, scale):
        def body(i, carry):
            at = pl.ds(pl.multiple_of(first + i * step, step), step)
            hid[at, :] = (x_norm[at, :] * scale + shift).astype(BF16)
            return carry

        lax.fori_loop(0, count // step, body, 0)

    modulate_rows(0, c_rows, vec(1), 1.0 + vec(3))
    modulate_rows(c_rows, rows, vec(0), 1.0 + vec(2))

    head_row = lax.broadcasted_iota(jnp.int32, (width, width), 0) // HEAD_DIM
    head_col = lax.broadcasted_iota(jnp.int32, (width, width), 1) // HEAD_DIM
    same_head = (head_row == head_col).astype(F32)

    def head_scale(p, gain):
        mean = jnp.dot(
            p * p, same_head, precision=lax.Precision.HIGHEST, preferred_element_type=F32
        ) * (1.0 / HEAD_DIM)
        wide_gain = jnp.concatenate([gain[...]] * heads, axis=1)
        return (p * lax.rsqrt(mean + EPS) * wide_gain).astype(BF16)

    own = pl.ds(rows + pl.multiple_of(side * rows, rows), rows)
    other = pl.ds(rows + pl.multiple_of((1 - side) * rows, rows), rows)

    def split(stage, value):
        for h in range(2):
            stage[h] = value[:, h * half : (h + 1) * half]

    def trade(index, stage, block_all, at):
        c = remote(
            stage.at[1 - side], block_all.at[at], pair_send.at[index], pair_recv.at[index],
            mate, me_t,
        )
        c.start()
        sends.append(c)
        return c

    def share_ctx(index, stage, block_ctx):
        block_ctx[me_s] = stage[side]
        for k in range(1, n_sp):
            peer = lax.rem(me_s + k, n_sp)
            c = remote(
                stage.at[lax.rem(peer, 2)], block_ctx.at[me_s],
                ctx_send.at[index, k], ctx_recv.at[index, me_s], peer, me_t,
            )
            c.start()
            sends.append(c)

    def halo_copies(index, block_all):
        down = remote(
            block_all.at[pl.ds(rows, rows)], block_all.at[pl.ds(3 * rows, rows)],
            halo_send.at[index, 0], halo_recv.at[index, 0], me_s - 2, me_t,
        )
        up = remote(
            block_all.at[pl.ds(2 * rows, rows)], block_all.at[pl.ds(0, rows)],
            halo_send.at[index, 1], halo_recv.at[index, 1], me_s + 2, me_t,
        )
        return down, up

    def halo_start(mine, index, block_all):
        down, up = halo_copies(index, block_all)
        is_low = side == 0 if mine else side == 1

        @pl.when(is_low & (slab > 0))
        def _():
            down.start()

        @pl.when(jnp.logical_not(is_low) & (slab < last_slab))
        def _():
            up.start()

    copies[5].wait()
    keys = head_scale(jnp.dot(hid[...], w_qkv[0], preferred_element_type=F32), key_gain)
    split(k_stage, keys[c_rows:])
    k_trade = trade(0, k_stage, k_all, own)
    k_all[own, :] = k_stage[side]
    halo_start(True, 0, k_all)
    split(ck_stage, keys[:c_rows])
    share_ctx(0, ck_stage, ctx_k)
    copies[6].wait()
    values = jnp.dot(hid[...], w_qkv[1], preferred_element_type=F32).astype(BF16)
    split(v_stage, values[c_rows:])
    v_trade = trade(1, v_stage, v_all, own)
    v_all[own, :] = v_stage[side]
    halo_start(True, 1, v_all)
    split(cv_stage, values[:c_rows])
    share_ctx(1, cv_stage, ctx_v)
    copies[7].wait()
    queries = head_scale(
        jnp.dot(hid[c_rows:, :], w_qkv[2], preferred_element_type=F32), query_gain
    ) * jnp.asarray(HEAD_DIM ** (-0.5), BF16)
    split(q_stage, queries)
    q_own = pl.ds(pl.multiple_of(side * rows, rows), rows)
    q_trade = trade(2, q_stage, q_all, q_own)
    q_all[q_own, :] = q_stage[side]
    k_trade.wait_recv()
    halo_start(False, 0, k_all)
    v_trade.wait_recv()
    halo_start(False, 1, v_all)
    gather_forward(wo_view(0), wo_sems(0))
    q_trade.wait_recv()

    for index, block_ctx in enumerate((ctx_k, ctx_v)):
        for k in range(1, n_sp):
            peer = lax.rem(me_s + k, n_sp)
            remote(
                block_ctx.at[peer], block_ctx.at[peer],
                ctx_send.at[index, k], ctx_recv.at[index, peer], peer, me_t,
            ).wait_recv()
    for index, block_all in enumerate((k_all, v_all)):
        down, up = halo_copies(index, block_all)

        @pl.when(slab < last_slab)
        def _():
            down.wait_recv()

        @pl.when(slab > 0)
        def _():
            up.wait_recv()

    lane_head = lax.broadcasted_iota(jnp.int32, (GRID_W, half), 1) // HEAD_DIM
    masks = [(lane_head == h).astype(F32) for h in range(half_heads)]
    contract_last = (((1,), (1,)), ((), ()))
    all_ck = ctx_k[...].reshape(n_sp * c_rows, half)
    all_cv = ctx_v[...].reshape(n_sp * c_rows, half)

    def attend(i):
        start = jnp.where(
            slab == 0,
            jnp.maximum(i, halo),
            jnp.where(slab == last_slab, jnp.minimum(i, halo), i),
        )
        if last_slab == 0:
            start = jnp.int32(halo)
        at = pl.ds(pl.multiple_of(start * GRID_W, GRID_W), win)
        row_at = pl.ds(pl.multiple_of(i * GRID_W, GRID_W), GRID_W)
        qi = q_all[row_at, :].astype(F32)
        qs = jnp.concatenate([(qi * m).astype(BF16) for m in masks], axis=0)
        s1 = lax.dot_general(qs, k_all[at, :], contract_last, preferred_element_type=F32)
        first = start - i + WIN_ROWS - 1 - halo
        s1 = s1 + jnp.concatenate([table[first + 2 * m] for m in range(WIN_ROWS // 2)], axis=1)
        s2 = lax.dot_general(qs, all_ck, contract_last, preferred_element_type=F32)
        top = jnp.maximum(
            jnp.max(s1, axis=1, keepdims=True), jnp.max(s2, axis=1, keepdims=True)
        )
        e1 = jnp.exp(s1 - top)
        e2 = jnp.exp(s2 - top)
        inv = 1.0 / (jnp.sum(e1, axis=1, keepdims=True) + jnp.sum(e2, axis=1, keepdims=True))
        o = jnp.dot((e1 * inv).astype(BF16), v_all[at, :], preferred_element_type=F32)
        o = o + jnp.dot((e2 * inv).astype(BF16), all_cv, preferred_element_type=F32)
        picked = o[:GRID_W] * masks[0]
        for h in range(1, half_heads):
            picked = picked + o[h * GRID_W : (h + 1) * GRID_W] * masks[h]
        return picked.astype(BF16)

    for i in range(l_rows):
        att_slab[i * GRID_W : (i + 1) * GRID_W, :] = attend((1 - side) * l_rows + i)
    back = remote(
        att_slab, att.at[me_t, side], pair_send.at[3], pair_recv.at[3], mate, me_t
    )
    back.start()
    sends.append(back)
    for i in range(l_rows):
        att[me_t, side, i * GRID_W : (i + 1) * GRID_W, :] = attend(side * l_rows + i)

    back_in = remote(
        att_slab, att.at[me_t, 1 - side], pair_send.at[3], pair_recv.at[3], mate, me_t
    )
    first, second = att_view(side), att_view(1 - side)
    gather_start(first, att_sems(0))
    back_in.wait_recv()
    gather_start(second, att_sems(1))
    gather_forward(first, att_sems(0))
    gather_forward(wo_view(1), wo_sems(1))
    gather_forward(second, att_sems(1))
    copies[8].wait()
    gather_finish(wo_view(0), wo_sems(0))
    gather_finish(wo_view(1), wo_sems(1))
    gather_finish(first, att_sems(0))
    gather_finish(second, att_sems(1))
    gate = vec(4)
    cols = 512
    for n in range(d // cols):
        at = slice(n * cols, (n + 1) * cols)
        branch = jnp.zeros((rows, cols), F32)
        for j in range(n_tp):
            branch = branch + jnp.dot(
                jnp.concatenate([att[j, 0], att[j, 1]], axis=1),
                w_out[j, :, at],
                preferred_element_type=F32,
            ).astype(BF16).astype(F32)
        base = x_in[c_rows:, at].astype(F32)
        out[:, at] = (base + gate[:, at] * branch).astype(BF16)

    for c in sends:
        c.wait_send()
    for index, block_all in enumerate((k_all, v_all)):
        down, up = halo_copies(index, block_all)

        @pl.when(slab > 0)
        def _():
            down.wait_send()

        @pl.when(slab < last_slab)
        def _():
            up.wait_send()


def per_device(
    latent,
    context,
    condition,
    ctx_condition,
    shift_weight,
    scale_weight,
    gate_weight,
    norm_gain,
    query_weight,
    key_weight,
    value_weight,
    query_gain,
    key_gain,
    offset_bias,
    out_weight,
):
    n_sp, n_tp = lax.axis_size("sp"), lax.axis_size("tp")
    rows, d = latent.shape
    c_rows = context.shape[0]
    width = key_weight.shape[1]
    heads = width // HEAD_DIM
    block = shift_weight.shape[1]
    n_pairs = 2 * WIN_ROWS - 2
    half = width // 2
    half_heads = heads // 2
    any_spec = pl.BlockSpec(memory_space=pl.ANY)
    vmem_spec = pl.BlockSpec(memory_space=pltpu.VMEM)
    dma = pltpu.SemaphoreType.DMA
    return pl.pallas_call(
        functools.partial(fused_kernel, n_sp, n_tp),
        out_shape=pltpu.VMEM((rows, d), BF16),
        in_specs=[any_spec] * 9 + [vmem_spec] * 6,
        out_specs=vmem_spec,
        scratch_shapes=[
            pltpu.VMEM((rows + c_rows, d), BF16),
            pltpu.VMEM((rows + c_rows, d), F32),
            pltpu.VMEM((rows + c_rows, d), BF16),
            pltpu.VMEM((3, shift_weight.shape[0], block), BF16),
            pltpu.VMEM((3, d, width), BF16),
            pltpu.VMEM((n_tp, width, d), BF16),
            pltpu.VMEM((n_sp, 8, block), F32),
            pltpu.VMEM((n_tp, 8, block), F32),
            pltpu.VMEM((2, rows, half), BF16),
            pltpu.VMEM((2, rows, half), BF16),
            pltpu.VMEM((2, rows, half), BF16),
            pltpu.VMEM((2, c_rows, half), BF16),
            pltpu.VMEM((2, c_rows, half), BF16),
            pltpu.VMEM((2 * rows, half), BF16),
            pltpu.VMEM((4 * rows, half), BF16),
            pltpu.VMEM((4 * rows, half), BF16),
            pltpu.VMEM((n_sp, c_rows, half), BF16),
            pltpu.VMEM((n_sp, c_rows, half), BF16),
            pltpu.VMEM((heads, 2 * WIN_ROWS, 2 * GRID_W), F32),
            pltpu.VMEM((half_heads, 2 * WIN_ROWS, 2 * GRID_W), F32),
            pltpu.VMEM((n_pairs, half_heads * GRID_W, 2 * GRID_W), F32),
            pltpu.VMEM((rows, half), BF16),
            pltpu.VMEM((n_tp, 2, rows, half), BF16),
            dma((9,)),
            dma((n_sp,)),
            dma((n_sp,)),
            dma((n_tp,)),
            dma((n_tp,)),
            dma((4,)),
            dma((4,)),
            dma((2, 2)),
            dma((2, 2)),
            dma((2, n_sp)),
            dma((2, n_sp)),
            dma((2, n_tp)),
            dma((2, n_tp)),
            dma((2, n_tp)),
            dma((2, n_tp)),
        ],
        compiler_params=pltpu.CompilerParams(collective_id=0, has_side_effects=True),
        name="fused_block",
    )(
        latent,
        context,
        shift_weight,
        scale_weight,
        gate_weight,
        query_weight,
        key_weight,
        value_weight,
        out_weight,
        condition.reshape(1, -1),
        ctx_condition.reshape(1, -1),
        norm_gain.reshape(1, -1),
        query_gain.reshape(1, -1),
        key_gain.reshape(1, -1),
        offset_bias.transpose(1, 0, 2),
    )


def fused_fits(latent, context, condition, query_weight, n_sp, n_tp):
    rows, c_rows = latent.shape[0] // n_sp, context.shape[0] // n_sp
    width = query_weight.shape[1] // n_tp
    return (
        rows == WIN_ROWS // 2 * GRID_W
        and c_rows % 32 == 0
        and condition.shape[0] // n_sp % 128 == 0
        and width % 256 == 0
        and n_tp % 2 == 0
        and n_sp % 2 == 0
    )


def solution(mesh):
    in_specs = (
        P("sp", None),
        P("sp", None),
        P("sp"),
        P("sp"),
        P("sp", "tp"),
        P("sp", "tp"),
        P("sp", "tp"),
        P(),
        P(None, "tp"),
        P(None, "tp"),
        P(None, "tp"),
        P(),
        P(),
        P("tp", None, None),
        P("tp", None),
    )
    out_specs = P("sp", None)

    def step(latent, context, condition, ctx_condition, *rest):
        n_sp, n_tp = mesh.shape["sp"], mesh.shape["tp"]
        fits = fused_fits(latent, context, condition, rest[4], n_sp, n_tp)
        body = per_device if fits else per_device_plain
        return jax.shard_map(
            body, mesh=mesh, in_specs=in_specs, out_specs=out_specs, check_vma=False
        )(latent, context, condition, ctx_condition, *rest)

    return step
```

profile of v0, /device:TPU:1, one launch (start us, length us, event | category | flops | bytes accessed | tf_op | source)
XLA Modules:
  0.0 40.4 jit_solution(16294485750186569423)
XLA Ops:
  0.0 39.4 %fused_block.1 = bf16[256,2048]{1,0:T(8,128)(2,1)S(1)} custom-call(bf16[256,2048]{1,0:T(8,128)(2,1)} %latent.1, bf16[64,2048]{1,0:T(8,128)(2,1)} %context.1, bf16[256,512]{1,0:T(8,128)(2,1)} %shift_w.1, bf16[256,512]{1,0:T(8,128)(2,1)} %scale_w.1, bf16[256,512]{1,0:T(8,128)(2,1)} %gate_w.1, bf16[2048,256]{1,0:T(8,128)(2,1)} %query_w.1, ...), custom_call_target="tpu_custom_call" | custom-call | tf_op jit(solution)/shard_map/fused_block/pallas_call | solution.py:665
  39.4 1.0 %copy.17 = bf16[256,2048]{1,0:T(8,128)(2,1)} copy(bf16[256,2048]{1,0:T(8,128)(2,1)S(1)} %fused_block.1) | data formatting | bytes 2097152
where the time goes:
time: 40.6 us; the launch traced here: 40.4 us
  Pallas kernels  39.4 us (97%)
  local copies, waits for them, and re-layouts  0.97 us (2%)
    pallas_call x1, Pallas kernels, per_device(): pl.pallas_call(functools.partial(fused_kernel, n_sp, n_tp), out_shape=plt...  39.4 us
    unnamed x1, local copies, waits for them, and re-layouts  0.97 us

commit v1 on v0

--- a/solution.py
+++ b/solution.py
@@ -193,6 +193,12 @@
     key_gain,
     bias_in,
     out,
+    cond_v,
+    ctx_cond_v,
+    norm_gain_v,
+    query_gain_v,
+    key_gain_v,
+    bias_v,
     x_in,
     x_norm,
     hid,
@@ -201,6 +207,9 @@
     w_out,
     mod_sp,
     mod_tp,
+    gate_sp,
+    gate_tp,
+    acc,
     q_stage,
     k_stage,
     v_stage,
@@ -221,6 +230,10 @@
     mod_recv,
     modt_send,
     modt_recv,
+    gate_send,
+    gate_recv,
+    gatet_send,
+    gatet_recv,
     pair_send,
     pair_recv,
     halo_send,
@@ -238,6 +251,7 @@
     width = key_w.shape[1]
     heads = width // HEAD_DIM
     block = shift_w.shape[1]
+    blocks = block // 128
     l_rows = rows // GRID_W
     halo = WIN_ROWS // 2
     win = WIN_ROWS * GRID_W
@@ -258,16 +272,6 @@
             device_id=(s, t), device_id_type=MESH,
         )
 
-    barrier = pltpu.get_barrier_semaphore()
-    for k in range(1, n_sp):
-        pl.semaphore_signal(
-            barrier, inc=1, device_id=(lax.rem(me_s + k, n_sp), me_t), device_id_type=MESH
-        )
-    for k in range(1, n_tp):
-        pl.semaphore_signal(
-            barrier, inc=1, device_id=(me_s, lax.rem(me_t + k, n_tp)), device_id_type=MESH
-        )
-
     loads = [
         (shift_w, w_mod.at[0]),
         (scale_w, w_mod.at[1]),
@@ -278,18 +282,36 @@
         (value_w, w_qkv.at[1]),
         (query_w, w_qkv.at[2]),
         (out_w, w_out.at[me_t]),
+        (cond, cond_v),
+        (ctx_cond, ctx_cond_v),
+        (norm_gain, norm_gain_v),
+        (query_gain, query_gain_v),
+        (key_gain, key_gain_v),
+        (bias_in, bias_v),
     ]
     copies = [pltpu.make_async_copy(a, b, local_sem.at[i]) for i, (a, b) in enumerate(loads)]
-    for c in copies[:3]:
-        c.start()
+    for i in (9, 10, 0, 1, 2, 11, 12, 13, 14, 3, 4):
+        copies[i].start()
+
+    barrier = pltpu.get_barrier_semaphore()
+    for k in range(1, n_sp):
+        pl.semaphore_signal(
+            barrier, inc=1, device_id=(lax.rem(me_s + k, n_sp), me_t), device_id_type=MESH
+        )
+    for k in range(1, n_tp):
+        pl.semaphore_signal(
+            barrier, inc=1, device_id=(me_s, lax.rem(me_t + k, n_tp)), device_id_type=MESH
+        )
 
     def silu(v):
         return v / (1.0 + jnp.exp(-v))
 
     two = (16, cond.shape[1])
     row_id = lax.broadcasted_iota(jnp.int32, two, 0)
-    act0 = jnp.broadcast_to(silu(cond[...]), two)
-    act1 = jnp.broadcast_to(silu(ctx_cond[...]), two)
+    copies[9].wait()
+    copies[10].wait()
+    act0 = jnp.broadcast_to(silu(cond_v[...]), two)
+    act1 = jnp.broadcast_to(silu(ctx_cond_v[...]), two)
 
     def placed(first, second):
         picked = jnp.where(row_id == first, act0, 0.0)
@@ -301,18 +323,43 @@
     for i, (first, second) in enumerate(((0, 1), (2, 3), (4, None))):
         copies[i].wait()
         part += jnp.dot(placed(first, second), w_mod[i], preferred_element_type=F32)
-    for c in copies[3:]:
-        c.start()
-    mod_sp[me_s] = part[:8]
+    for b in range(blocks):
+        mod_sp[me_s, 4 * b : 4 * b + 4, :] = part[:4, b * 128 : (b + 1) * 128]
+        gate_sp[me_s, b : b + 1, :] = part[4:5, b * 128 : (b + 1) * 128]
     pl.semaphore_wait(barrier, n_sp + n_tp - 2)
     sends = []
-    for k in range(1, n_sp):
-        peer = lax.rem(me_s + k, n_sp)
-        c = remote(
-            mod_sp.at[me_s], mod_sp.at[me_s], mod_send.at[k], mod_recv.at[me_s], peer, me_t
-        )
-        c.start()
-        sends.append(c)
+
+    def share_sp(buf, send, recv):
+        for k in range(1, n_sp):
+            peer = lax.rem(me_s + k, n_sp)
+            c = remote(buf.at[me_s], buf.at[me_s], send.at[k], recv.at[me_s], peer, me_t)
+            c.start()
+            sends.append(c)
+
+    def sum_sp(buf, send, recv):
+        for k in range(1, n_sp):
+            peer = lax.rem(me_s + k, n_sp)
+            remote(buf.at[peer], buf.at[peer], send.at[k], recv.at[peer], peer, me_t).wait_recv()
+        total = buf[0]
+        for k in range(1, n_sp):
+            total = total + buf[k]
+        return total
+
+    def share_tp(buf, send, recv):
+        for k in range(1, n_tp):
+            peer = lax.rem(me_t + k, n_tp)
+            c = remote(buf.at[me_t], buf.at[me_t], send.at[k], recv.at[me_t], me_s, peer)
+            c.start()
+            sends.append(c)
+
+    def wait_tp(buf, send, recv):
+        for k in range(1, n_tp):
+            peer = lax.rem(me_t + k, n_tp)
+            remote(buf.at[peer], buf.at[peer], send.at[k], recv.at[peer], me_s, peer).wait_recv()
+
+    share_sp(mod_sp, mod_send, mod_recv)
+    for i in (5, 6, 7, 8):
+        copies[i].start()
 
     def gather_start(view, sems, source=None):
         send, recv = sems
@@ -334,28 +381,62 @@
             c.start()
             sends.append(c)
 
-    def gather_finish(view, sems):
-        send, recv = sems
-        remote(
-            view(partner), view(partner), send(0), recv(partner), me_s, partner
-        ).wait_recv()
-        for k in range(1, n_x):
-            came = 2 * lax.rem(chip + n_x - k, n_x) + 1 - core
-            remote(
-                view(came), view(came), send(n_x + k), recv(came), me_s, partner
+    far = 2 * (1 - chip) + core
+    far_partner = 2 * (1 - chip) + 1 - core
+    piece = width // 8
+    y_pieces = 2
+    direct = width - 2 * y_pieces * piece
+
+    def wo_rows(c, at_side):
+        if c < y_pieces:
+            start = direct + at_side * y_pieces * piece + c * piece
+        else:
+            start = (c - y_pieces) * piece
+        return pl.ds(pl.multiple_of(start, piece), piece)
+
+    n_pieces = direct // piece + y_pieces
+
+    def wo_copy(kind, c, source, shard, rows_at, s, t):
+        return remote(
+            source.at[rows_at], w_out.at[shard, rows_at],
+            wo_send.at[kind, c], wo_recv.at[kind, c], s, t,
+        )
+
+    def begin(c):
+        c.start()
+        sends.append(c)
+
+    def wo_far(c):
+        return wo_copy(0, c, out_w, me_t, wo_rows(c, side), me_s, far)
+
+    def wo_forward(c):
+        at_rows = wo_rows(c, side)
+        came = w_out.at[far]
+        wo_copy(0, c, came, far, at_rows, me_s, far).wait_recv()
+        begin(wo_copy(1, c, came, far, at_rows, me_s, partner))
+        if c < y_pieces:
+            begin(wo_copy(2, c, came, far, at_rows, mate, me_t))
+
+    def wo_cross(c):
+        at_rows = wo_rows(c, 1 - side)
+        came = w_out.at[far]
+        wo_copy(2, c, came, far, at_rows, mate, me_t).wait_recv()
+        begin(wo_copy(3, c, came, far, at_rows, me_s, partner))
+
+    def wo_finish_far():
+        for c in range(n_pieces):
+            wo_copy(
+                1, c, w_out.at[far_partner], far_partner, wo_rows(c, side), me_s, partner
             ).wait_recv()
-
-    early = width // 4
-    wo_rows = (pl.ds(0, early), pl.ds(early, width - early))
-
-    def wo_view(c):
-        return lambda j: w_out.at[j, wo_rows[c]]
-
-    def wo_source(c):
-        return out_w.at[wo_rows[c]]
-
-    def wo_sems(c):
-        return (lambda k: wo_send.at[c, k]), (lambda k: wo_recv.at[c, k])
+        for c in range(y_pieces):
+            wo_copy(
+                3, c, w_out.at[far_partner], far_partner, wo_rows(c, 1 - side), me_s, partner
+            ).wait_recv()
+
+    def wo_partner():
+        return remote(
+            out_w, w_out.at[me_t], wo_send.at[4, 0], wo_recv.at[4, 0], me_s, partner
+        )
 
     def att_view(h):
         return lambda j: att.at[j, h]
@@ -363,17 +444,18 @@
     def att_sems(n):
         return (lambda k: att_send.at[n, k]), (lambda k: att_recv.at[n, k])
 
-    gather_start(wo_view(0), wo_sems(0), wo_source(0))
+    begin(wo_far(0))
 
     copies[3].wait()
     copies[4].wait()
+    copies[11].wait()
     step = 32
 
     def norm_rows(i, carry):
         at = pl.ds(pl.multiple_of(i * step, step), step)
         v = x_in[at, :].astype(F32)
         r = lax.rsqrt(jnp.mean(v * v, axis=-1, keepdims=True) + EPS)
-        x_norm[at, :] = v * r * norm_gain[...]
+        x_norm[at, :] = v * r * norm_gain_v[...]
         return carry
 
     lax.fori_loop(0, (rows + c_rows) // step, norm_rows, 0)
@@ -384,9 +466,10 @@
     col0 = jnp.clip(q_col - WIN_COLS // 2, 0, GRID_W - WIN_COLS)
     col_open = (k_col >= col0) & (k_col < col0 + WIN_COLS)
     n_pairs = 2 * WIN_ROWS - 2
+    copies[14].wait()
     bias_pad[...] = jnp.zeros_like(bias_pad)
     for h in range(heads):
-        bias_pad[h, : 2 * WIN_ROWS - 1, : 2 * WIN_COLS - 1] = bias_in[:, h, :]
+        bias_pad[h, : 2 * WIN_ROWS - 1, : 2 * WIN_COLS - 1] = bias_v[:, h, :]
     for h in range(half_heads):
         head = side * half_heads + h
         upper = pltpu.roll(bias_pad[head, 1 : n_pairs + 1, :], GRID_W, 1)
@@ -396,33 +479,19 @@
             rolled = pltpu.roll(line, pair - (WIN_COLS - 1), 1, stride=1, stride_axis=0)
             table[a, h * GRID_W : (h + 1) * GRID_W, :] = jnp.where(col_open, rolled, MASKED)
 
-    for k in range(1, n_sp):
-        peer = lax.rem(me_s + k, n_sp)
-        remote(
-            mod_sp.at[peer], mod_sp.at[peer], mod_send.at[k], mod_recv.at[peer], peer, me_t
-        ).wait_recv()
-    total = mod_sp[0]
-    for k in range(1, n_sp):
-        total = total + mod_sp[k]
-    mod_tp[me_t] = total
-    for k in range(1, n_tp):
-        peer = lax.rem(me_t + k, n_tp)
-        c = remote(
-            mod_tp.at[me_t], mod_tp.at[me_t], modt_send.at[k], modt_recv.at[me_t], me_s, peer
-        )
-        c.start()
-        sends.append(c)
-
-    gather_start(wo_view(1), wo_sems(1), wo_source(1))
-
-    for k in range(1, n_tp):
-        peer = lax.rem(me_t + k, n_tp)
-        remote(
-            mod_tp.at[peer], mod_tp.at[peer], modt_send.at[k], modt_recv.at[peer], me_s, peer
-        ).wait_recv()
+    mod_tp[me_t] = sum_sp(mod_sp, mod_send, mod_recv)
+    share_tp(mod_tp, modt_send, modt_recv)
+    begin(wo_partner())
+    share_sp(gate_sp, gate_send, gate_recv)
+    wait_tp(mod_tp, modt_send, modt_recv)
+    for c in range(1, n_pieces):
+        begin(wo_far(c))
 
     def vec(r):
-        return jnp.concatenate([mod_tp[j][r : r + 1, :] for j in range(n_tp)], axis=1)
+        return jnp.concatenate(
+            [mod_tp[j, 4 * b + r : 4 * b + r + 1, :] for j in range(n_tp) for b in range(blocks)],
+            axis=1,
+        )
 
     def modulate_rows(first, count, shift, scale):
         def body(i, carry):
@@ -437,12 +506,17 @@
 
     head_row = lax.broadcasted_iota(jnp.int32, (width, width), 0) // HEAD_DIM
     head_col = lax.broadcasted_iota(jnp.int32, (width, width), 1) // HEAD_DIM
-    same_head = (head_row == head_col).astype(F32)
+    same_head = (head_row == head_col).astype(BF16)
+    copies[12].wait()
+    copies[13].wait()
 
     def head_scale(p, gain):
-        mean = jnp.dot(
-            p * p, same_head, precision=lax.Precision.HIGHEST, preferred_element_type=F32
-        ) * (1.0 / HEAD_DIM)
+        squares = p * p
+        high = squares.astype(BF16)
+        low = (squares - high.astype(F32)).astype(BF16)
+        mean = jnp.dot(high, same_head, preferred_element_type=F32)
+        mean = mean + jnp.dot(low, same_head, preferred_element_type=F32)
+        mean = mean * (1.0 / HEAD_DIM)
         wide_gain = jnp.concatenate([gain[...]] * heads, axis=1)
         return (p * lax.rsqrt(mean + EPS) * wide_gain).astype(BF16)
 
@@ -497,7 +571,7 @@
             up.start()
 
     copies[5].wait()
-    keys = head_scale(jnp.dot(hid[...], w_qkv[0], preferred_element_type=F32), key_gain)
+    keys = head_scale(jnp.dot(hid[...], w_qkv[0], preferred_element_type=F32), key_gain_v)
     split(k_stage, keys[c_rows:])
     k_trade = trade(0, k_stage, k_all, own)
     k_all[own, :] = k_stage[side]
@@ -514,17 +588,19 @@
     share_ctx(1, cv_stage, ctx_v)
     copies[7].wait()
     queries = head_scale(
-        jnp.dot(hid[c_rows:, :], w_qkv[2], preferred_element_type=F32), query_gain
+        jnp.dot(hid[c_rows:, :], w_qkv[2], preferred_element_type=F32), query_gain_v
     ) * jnp.asarray(HEAD_DIM ** (-0.5), BF16)
     split(q_stage, queries)
     q_own = pl.ds(pl.multiple_of(side * rows, rows), rows)
     q_trade = trade(2, q_stage, q_all, q_own)
     q_all[q_own, :] = q_stage[side]
+    gate_tp[me_t] = sum_sp(gate_sp, gate_send, gate_recv)
+    share_tp(gate_tp, gatet_send, gatet_recv)
+    wo_forward(0)
     k_trade.wait_recv()
     halo_start(False, 0, k_all)
     v_trade.wait_recv()
     halo_start(False, 1, v_all)
-    gather_forward(wo_view(0), wo_sems(0))
     q_trade.wait_recv()
 
     for index, block_ctx in enumerate((ctx_k, ctx_v)):
@@ -587,6 +663,7 @@
     )
     back.start()
     sends.append(back)
+    wo_forward(1)
     for i in range(l_rows):
         att[me_t, side, i * GRID_W : (i + 1) * GRID_W, :] = attend(side * l_rows + i)
 
@@ -597,27 +674,58 @@
     gather_start(first, att_sems(0))
     back_in.wait_recv()
     gather_start(second, att_sems(1))
+    for c in range(2, n_pieces):
+        wo_forward(c)
+    for c in range(y_pieces):
+        wo_cross(c)
+    wait_tp(gate_tp, gatet_send, gatet_recv)
+    gate = jnp.concatenate(
+        [gate_tp[j, b : b + 1, :] for j in range(n_tp) for b in range(blocks)], axis=1
+    )
+    copies[8].wait()
+    cols = 512
+
+    def project(j, first_group, last_group):
+        heads_of = jnp.concatenate([att[j, 0], att[j, 1]], axis=1)
+        for n in range(d // cols):
+            at = slice(n * cols, (n + 1) * cols)
+            term = jnp.dot(heads_of, w_out[j, :, at], preferred_element_type=F32)
+            term = term.astype(BF16).astype(F32)
+            if not first_group:
+                term = acc[:, at] + term
+            if last_group:
+                base = x_in[c_rows:, at].astype(F32)
+                out[:, at] = (base + gate[:, at] * term).astype(BF16)
+            else:
+                acc[:, at] = term
+
+    project(me_t, True, False)
     gather_forward(first, att_sems(0))
-    gather_forward(wo_view(1), wo_sems(1))
     gather_forward(second, att_sems(1))
-    copies[8].wait()
-    gather_finish(wo_view(0), wo_sems(0))
-    gather_finish(wo_view(1), wo_sems(1))
-    gather_finish(first, att_sems(0))
-    gather_finish(second, att_sems(1))
-    gate = vec(4)
-    cols = 512
-    for n in range(d // cols):
-        at = slice(n * cols, (n + 1) * cols)
-        branch = jnp.zeros((rows, cols), F32)
-        for j in range(n_tp):
-            branch = branch + jnp.dot(
-                jnp.concatenate([att[j, 0], att[j, 1]], axis=1),
-                w_out[j, :, at],
-                preferred_element_type=F32,
-            ).astype(BF16).astype(F32)
-        base = x_in[c_rows:, at].astype(F32)
-        out[:, at] = (base + gate[:, at] * branch).astype(BF16)
+    remote(
+        w_out.at[partner], w_out.at[partner], wo_send.at[4, 0], wo_recv.at[4, 0], me_s, partner
+    ).wait_recv()
+
+    def att_wait(view, sems):
+        send, recv = sems
+        remote(
+            view(partner), view(partner), send(0), recv(partner), me_s, partner
+        ).wait_recv()
+
+    def att_wait_far(view, sems):
+        send, recv = sems
+        remote(
+            view(far_partner), view(far_partner), send(n_x + 1), recv(far_partner), me_s, partner
+        ).wait_recv()
+
+    att_wait(first, att_sems(0))
+    att_wait(second, att_sems(1))
+    project(partner, False, False)
+    project(far, False, False)
+    wo_finish_far()
+    att_wait_far(first, att_sems(0))
+    att_wait_far(second, att_sems(1))
+    project(far_partner, False, True)
 
     for c in sends:
         c.wait_send()
@@ -659,23 +767,33 @@
     n_pairs = 2 * WIN_ROWS - 2
     half = width // 2
     half_heads = heads // 2
+    blocks = block // 128
     any_spec = pl.BlockSpec(memory_space=pl.ANY)
     vmem_spec = pl.BlockSpec(memory_space=pltpu.VMEM)
     dma = pltpu.SemaphoreType.DMA
     return pl.pallas_call(
         functools.partial(fused_kernel, n_sp, n_tp),
         out_shape=pltpu.VMEM((rows, d), BF16),
-        in_specs=[any_spec] * 9 + [vmem_spec] * 6,
+        in_specs=[any_spec] * 15,
         out_specs=vmem_spec,
         scratch_shapes=[
+            pltpu.VMEM((1, condition.shape[0]), F32),
+            pltpu.VMEM((1, condition.shape[0]), F32),
+            pltpu.VMEM((1, d), F32),
+            pltpu.VMEM((1, HEAD_DIM), F32),
+            pltpu.VMEM((1, HEAD_DIM), F32),
+            pltpu.VMEM((2 * WIN_ROWS - 1, heads, 2 * WIN_COLS - 1), F32),
             pltpu.VMEM((rows + c_rows, d), BF16),
             pltpu.VMEM((rows + c_rows, d), F32),
             pltpu.VMEM((rows + c_rows, d), BF16),
             pltpu.VMEM((3, shift_weight.shape[0], block), BF16),
             pltpu.VMEM((3, d, width), BF16),
             pltpu.VMEM((n_tp, width, d), BF16),
-            pltpu.VMEM((n_sp, 8, block), F32),
-            pltpu.VMEM((n_tp, 8, block), F32),
+            pltpu.VMEM((n_sp, 4 * blocks, 128), F32),
+            pltpu.VMEM((n_tp, 4 * blocks, 128), F32),
+            pltpu.VMEM((n_sp, blocks, 128), F32),
+            pltpu.VMEM((n_tp, blocks, 128), F32),
+            pltpu.VMEM((rows, d), F32),
             pltpu.VMEM((2, rows, half), BF16),
             pltpu.VMEM((2, rows, half), BF16),
             pltpu.VMEM((2, rows, half), BF16),
@@ -691,7 +809,11 @@
             pltpu.VMEM((n_pairs, half_heads * GRID_W, 2 * GRID_W), F32),
             pltpu.VMEM((rows, half), BF16),
             pltpu.VMEM((n_tp, 2, rows, half), BF16),
-            dma((9,)),
+            dma((15,)),
+            dma((n_sp,)),
+            dma((n_sp,)),
+            dma((n_tp,)),
+            dma((n_tp,)),
             dma((n_sp,)),
             dma((n_sp,)),
             dma((n_tp,)),
@@ -702,8 +824,8 @@
             dma((2, 2)),
             dma((2, n_sp)),
             dma((2, n_sp)),
-            dma((2, n_tp)),
-            dma((2, n_tp)),
+            dma((5, 8)),
+            dma((5, 8)),
             dma((2, n_tp)),
             dma((2, n_tp)),
         ],
@@ -735,8 +857,10 @@
         rows == WIN_ROWS // 2 * GRID_W
         and c_rows % 32 == 0
         and condition.shape[0] // n_sp % 128 == 0
+        and condition.shape[0] // n_tp % 256 == 0
+        and condition.shape[0] // n_tp <= 1024
         and width % 256 == 0
-        and n_tp % 2 == 0
+        and n_tp == 4
         and n_sp % 2 == 0
     )
 

time: 40.6 us -> 37.6 us (0.926)
  Pallas kernels: 39.4 us -> 36.3 us
    pallas_call x1, Pallas kernels: 39.4 us -> 36.3 us  [per_device(): pl.pallas_call(functools.partial(fused_kernel, n_sp, n_tp), out_shape=plt...]
where the time goes in v1:
time: 37.6 us; the launch traced here: 37.3 us
  Pallas kernels  36.3 us (97%)
  local copies, waits for them, and re-layouts  0.97 us (3%)
    pallas_call x1, Pallas kernels, per_device(): pl.pallas_call(functools.partial(fused_kernel, n_sp, n_tp), out_shape=plt...  36.3 us
    unnamed x1, local copies, waits for them, and re-layouts  0.97 us

profile of v1, /device:TPU:1, one launch (start us, length us, event | category | flops | bytes accessed | tf_op | source)
XLA Modules:
  0.0 37.3 jit_solution(6427985049699562144)
XLA Ops:
  0.0 36.3 %fused_block.1 = bf16[256,2048]{1,0:T(8,128)(2,1)S(1)} custom-call(bf16[256,2048]{1,0:T(8,128)(2,1)} %latent.1, bf16[64,2048]{1,0:T(8,128)(2,1)} %context.1, bf16[256,512]{1,0:T(8,128)(2,1)} %shift_w.1, bf16[256,512]{1,0:T(8,128)(2,1)} %scale_w.1, bf16[256,512]{1,0:T(8,128)(2,1)} %gate_w.1, bf16[2048,256]{1,0:T(8,128)(2,1)} %query_w.1, ...), custom_call_target="tpu_custom_call" | custom-call | tf_op jit(solution)/shard_map/fused_block/pallas_call | solution.py:774
  36.3 1.0 %copy.17 = bf16[256,2048]{1,0:T(8,128)(2,1)} copy(bf16[256,2048]{1,0:T(8,128)(2,1)S(1)} %fused_block.1) | data formatting | bytes 2097152

commit v2 on v1

--- a/solution.py
+++ b/solution.py
@@ -170,6 +170,7 @@
 
 MESH = pl.DeviceIdType.MESH
 MASKED = -1e30
+LANES = 128
 F32 = jnp.float32
 BF16 = jnp.bfloat16
 
@@ -207,6 +208,8 @@
     w_out,
     mod_sp,
     mod_tp,
+    part_kv,
+    part_q,
     gate_sp,
     gate_tp,
     acc,
@@ -223,6 +226,13 @@
     bias_pad,
     bias_lines,
     table,
+    q_heads,
+    scores,
+    tops,
+    sums,
+    scores_ctx,
+    weights,
+    sums_ctx,
     att_slab,
     att,
     local_sem,
@@ -258,7 +268,8 @@
     core = lax.rem(me_t, 2)
     chip = lax.div(me_t, 2)
     partner = me_t + 1 - 2 * core
-    n_x = n_tp // 2
+    far = 2 * (1 - chip) + core
+    far_partner = 2 * (1 - chip) + 1 - core
     side = lax.rem(me_s, 2)
     slab = lax.div(me_s, 2)
     mate = me_s + 1 - 2 * side
@@ -278,9 +289,9 @@
         (gate_w, w_mod.at[2]),
         (context, x_in.at[pl.ds(0, c_rows)]),
         (latent, x_in.at[pl.ds(c_rows, rows)]),
-        (key_w, w_qkv.at[0]),
-        (value_w, w_qkv.at[1]),
-        (query_w, w_qkv.at[2]),
+        (key_w, w_qkv.at[:, pl.ds(0, width)]),
+        (value_w, w_qkv.at[:, pl.ds(width, width)]),
+        (query_w, w_qkv.at[:, pl.ds(2 * width, width)]),
         (out_w, w_out.at[me_t]),
         (cond, cond_v),
         (ctx_cond, ctx_cond_v),
@@ -302,6 +313,7 @@
         pl.semaphore_signal(
             barrier, inc=1, device_id=(me_s, lax.rem(me_t + k, n_tp)), device_id_type=MESH
         )
+    pl.semaphore_signal(barrier, inc=1, device_id=(mate, far), device_id_type=MESH)
 
     def silu(v):
         return v / (1.0 + jnp.exp(-v))
@@ -320,13 +332,12 @@
         return picked.astype(BF16)
 
     part = jnp.zeros((16, block), F32)
-    for i, (first, second) in enumerate(((0, 1), (2, 3), (4, None))):
+    for i in range(2):
         copies[i].wait()
-        part += jnp.dot(placed(first, second), w_mod[i], preferred_element_type=F32)
+        part += jnp.dot(placed(2 * i, 2 * i + 1), w_mod[i], preferred_element_type=F32)
     for b in range(blocks):
         mod_sp[me_s, 4 * b : 4 * b + 4, :] = part[:4, b * 128 : (b + 1) * 128]
-        gate_sp[me_s, b : b + 1, :] = part[4:5, b * 128 : (b + 1) * 128]
-    pl.semaphore_wait(barrier, n_sp + n_tp - 2)
+    pl.semaphore_wait(barrier, n_sp + n_tp - 1)
     sends = []
 
     def share_sp(buf, send, recv):
@@ -360,29 +371,11 @@
     share_sp(mod_sp, mod_send, mod_recv)
     for i in (5, 6, 7, 8):
         copies[i].start()
-
-    def gather_start(view, sems, source=None):
-        send, recv = sems
-        mine = view(me_t) if source is None else source
-        started = [remote(mine, view(me_t), send(0), recv(me_t), me_s, partner)]
-        for k in range(1, n_x):
-            far = 2 * lax.rem(chip + k, n_x) + core
-            started.append(remote(mine, view(me_t), send(k), recv(me_t), me_s, far))
-        for c in reversed(started):
-            c.start()
-        sends.extend(started)
-
-    def gather_forward(view, sems):
-        send, recv = sems
-        for k in range(1, n_x):
-            came = 2 * lax.rem(chip + n_x - k, n_x) + core
-            c = remote(view(came), view(came), send(n_x + k), recv(came), me_s, partner)
-            c.wait_recv()
-            c.start()
-            sends.append(c)
-
-    far = 2 * (1 - chip) + core
-    far_partner = 2 * (1 - chip) + 1 - core
+    copies[2].wait()
+    gate_part = jnp.dot(placed(0, None), w_mod[2], preferred_element_type=F32)
+    for b in range(blocks):
+        gate_sp[me_s, b : b + 1, :] = gate_part[:1, b * 128 : (b + 1) * 128]
+
     piece = width // 8
     y_pieces = 2
     direct = width - 2 * y_pieces * piece
@@ -437,12 +430,6 @@
         return remote(
             out_w, w_out.at[me_t], wo_send.at[4, 0], wo_recv.at[4, 0], me_s, partner
         )
-
-    def att_view(h):
-        return lambda j: att.at[j, h]
-
-    def att_sems(n):
-        return (lambda k: att_send.at[n, k]), (lambda k: att_recv.at[n, k])
 
     begin(wo_far(0))
 
@@ -481,28 +468,58 @@
 
     mod_tp[me_t] = sum_sp(mod_sp, mod_send, mod_recv)
     share_tp(mod_tp, modt_send, modt_recv)
-    begin(wo_partner())
-    share_sp(gate_sp, gate_send, gate_recv)
-    wait_tp(mod_tp, modt_send, modt_recv)
     for c in range(1, n_pieces):
         begin(wo_far(c))
-
-    def vec(r):
+    share_sp(gate_sp, gate_send, gate_recv)
+
+    def wait_mod(peer):
+        remote(
+            mod_tp.at[peer], mod_tp.at[peer], modt_send.at[1], modt_recv.at[peer], me_s, peer
+        ).wait_recv()
+
+    pair_cols = 2 * block
+
+    def vec(which, r):
         return jnp.concatenate(
-            [mod_tp[j, 4 * b + r : 4 * b + r + 1, :] for j in range(n_tp) for b in range(blocks)],
+            [
+                mod_tp[2 * which + j, 4 * b + r : 4 * b + r + 1, :]
+                for j in range(2)
+                for b in range(blocks)
+            ],
             axis=1,
         )
 
-    def modulate_rows(first, count, shift, scale):
+    def cols_of(which):
+        return pl.ds(pl.multiple_of(which * pair_cols, pair_cols), pair_cols)
+
+    def modulate_rows(which, first, count, shift, scale):
         def body(i, carry):
             at = pl.ds(pl.multiple_of(first + i * step, step), step)
-            hid[at, :] = (x_norm[at, :] * scale + shift).astype(BF16)
+            hid[at, cols_of(which)] = (x_norm[at, cols_of(which)] * scale + shift).astype(BF16)
             return carry
 
         lax.fori_loop(0, count // step, body, 0)
 
-    modulate_rows(0, c_rows, vec(1), 1.0 + vec(3))
-    modulate_rows(c_rows, rows, vec(0), 1.0 + vec(2))
+    def modulate_pair(which):
+        modulate_rows(which, 0, c_rows, vec(which, 1), 1.0 + vec(which, 3))
+        modulate_rows(which, c_rows, rows, vec(which, 0), 1.0 + vec(which, 2))
+
+    def hidden_dot(which, start_row, start_col, count_col):
+        return jnp.dot(
+            hid[start_row:, cols_of(which)],
+            w_qkv[cols_of(which), start_col : start_col + count_col],
+            preferred_element_type=F32,
+        )
+
+    wait_mod(partner)
+    modulate_pair(chip)
+    for i in (5, 6, 7):
+        copies[i].wait()
+    part_kv[...] = hidden_dot(chip, 0, 0, 2 * width)
+    part_q[...] = hidden_dot(chip, c_rows, 2 * width, width)
+    wait_mod(far)
+    wait_mod(far_partner)
+    modulate_pair(1 - chip)
 
     head_row = lax.broadcasted_iota(jnp.int32, (width, width), 0) // HEAD_DIM
     head_col = lax.broadcasted_iota(jnp.int32, (width, width), 1) // HEAD_DIM
@@ -536,20 +553,29 @@
         sends.append(c)
         return c
 
-    def share_ctx(index, stage, block_ctx):
-        block_ctx[me_s] = stage[side]
-        for k in range(1, n_sp):
-            peer = lax.rem(me_s + k, n_sp)
-            c = remote(
-                stage.at[lax.rem(peer, 2)], block_ctx.at[me_s],
-                ctx_send.at[index, k], ctx_recv.at[index, me_s], peer, me_t,
-            )
-            c.start()
-            sends.append(c)
+    n_z = n_sp // 2
+    z_order = tuple(range(2, n_z)) + (1,)
+
+    def ctx_copy(index, slot, source, shard, block_ctx, s):
+        return remote(
+            source, block_ctx.at[shard], ctx_send.at[index, slot], ctx_recv.at[index, shard],
+            s, me_t,
+        )
+
+    def along_z(index, slot, source, shard, block_ctx):
+        for k in z_order:
+            peer = 2 * lax.rem(slab + k, n_z) + side
+            begin(ctx_copy(index, slot + k, source, shard, block_ctx, peer))
+
+    def relay_ctx(index, block_ctx):
+        ctx_copy(index, 0, block_ctx.at[mate], mate, block_ctx, mate).wait_recv()
+        along_z(index, n_z - 1, block_ctx.at[mate], mate, block_ctx)
+
+    lower = rows - GRID_W
 
     def halo_copies(index, block_all):
         down = remote(
-            block_all.at[pl.ds(rows, rows)], block_all.at[pl.ds(3 * rows, rows)],
+            block_all.at[pl.ds(rows, lower)], block_all.at[pl.ds(3 * rows, lower)],
             halo_send.at[index, 0], halo_recv.at[index, 0], me_s - 2, me_t,
         )
         up = remote(
@@ -570,46 +596,44 @@
         def _():
             up.start()
 
-    copies[5].wait()
-    keys = head_scale(jnp.dot(hid[...], w_qkv[0], preferred_element_type=F32), key_gain_v)
+    both = part_kv[...] + hidden_dot(1 - chip, 0, 0, 2 * width)
+    keys = head_scale(both[:, :width], key_gain_v)
+    split(ck_stage, keys[:c_rows])
     split(k_stage, keys[c_rows:])
+    begin(ctx_copy(0, 0, ck_stage.at[1 - side], me_s, ctx_k, mate))
     k_trade = trade(0, k_stage, k_all, own)
     k_all[own, :] = k_stage[side]
     halo_start(True, 0, k_all)
-    split(ck_stage, keys[:c_rows])
-    share_ctx(0, ck_stage, ctx_k)
-    copies[6].wait()
-    values = jnp.dot(hid[...], w_qkv[1], preferred_element_type=F32).astype(BF16)
+    along_z(0, 0, ck_stage.at[side], me_s, ctx_k)
+    ctx_k[me_s] = ck_stage[side]
+    values = both[:, width:].astype(BF16)
+    split(cv_stage, values[:c_rows])
     split(v_stage, values[c_rows:])
+    begin(ctx_copy(1, 0, cv_stage.at[1 - side], me_s, ctx_v, mate))
     v_trade = trade(1, v_stage, v_all, own)
     v_all[own, :] = v_stage[side]
     halo_start(True, 1, v_all)
-    split(cv_stage, values[:c_rows])
-    share_ctx(1, cv_stage, ctx_v)
-    copies[7].wait()
+    along_z(1, 0, cv_stage.at[side], me_s, ctx_v)
+    ctx_v[me_s] = cv_stage[side]
     queries = head_scale(
-        jnp.dot(hid[c_rows:, :], w_qkv[2], preferred_element_type=F32), query_gain_v
+        part_q[...] + hidden_dot(1 - chip, c_rows, 2 * width, width), query_gain_v
     ) * jnp.asarray(HEAD_DIM ** (-0.5), BF16)
     split(q_stage, queries)
     q_own = pl.ds(pl.multiple_of(side * rows, rows), rows)
     q_trade = trade(2, q_stage, q_all, q_own)
     q_all[q_own, :] = q_stage[side]
+    begin(wo_partner())
     gate_tp[me_t] = sum_sp(gate_sp, gate_send, gate_recv)
     share_tp(gate_tp, gatet_send, gatet_recv)
-    wo_forward(0)
+    relay_ctx(0, ctx_k)
+    relay_ctx(1, ctx_v)
+    for c in range(y_pieces):
+        wo_forward(c)
     k_trade.wait_recv()
     halo_start(False, 0, k_all)
     v_trade.wait_recv()
     halo_start(False, 1, v_all)
     q_trade.wait_recv()
-
-    for index, block_ctx in enumerate((ctx_k, ctx_v)):
-        for k in range(1, n_sp):
-            peer = lax.rem(me_s + k, n_sp)
-            remote(
-                block_ctx.at[peer], block_ctx.at[peer],
-                ctx_send.at[index, k], ctx_recv.at[index, peer], peer, me_t,
-            ).wait_recv()
     for index, block_all in enumerate((k_all, v_all)):
         down, up = halo_copies(index, block_all)
 
@@ -624,10 +648,11 @@
     lane_head = lax.broadcasted_iota(jnp.int32, (GRID_W, half), 1) // HEAD_DIM
     masks = [(lane_head == h).astype(F32) for h in range(half_heads)]
     contract_last = (((1,), (1,)), ((), ()))
-    all_ck = ctx_k[...].reshape(n_sp * c_rows, half)
-    all_cv = ctx_v[...].reshape(n_sp * c_rows, half)
-
-    def attend(i):
+    stack = half_heads * GRID_W
+    n_local = 2 * l_rows
+    ones = jnp.ones((win, 128), BF16)
+
+    def score_local(i):
         start = jnp.where(
             slab == 0,
             jnp.maximum(i, halo),
@@ -636,45 +661,95 @@
         if last_slab == 0:
             start = jnp.int32(halo)
         at = pl.ds(pl.multiple_of(start * GRID_W, GRID_W), win)
-        row_at = pl.ds(pl.multiple_of(i * GRID_W, GRID_W), GRID_W)
-        qi = q_all[row_at, :].astype(F32)
+        qi = q_all[i * GRID_W : (i + 1) * GRID_W, :].astype(F32)
         qs = jnp.concatenate([(qi * m).astype(BF16) for m in masks], axis=0)
-        s1 = lax.dot_general(qs, k_all[at, :], contract_last, preferred_element_type=F32)
+        q_heads[i] = qs
+        s = lax.dot_general(qs, k_all[at, :], contract_last, preferred_element_type=F32)
         first = start - i + WIN_ROWS - 1 - halo
-        s1 = s1 + jnp.concatenate([table[first + 2 * m] for m in range(WIN_ROWS // 2)], axis=1)
-        s2 = lax.dot_general(qs, all_ck, contract_last, preferred_element_type=F32)
-        top = jnp.maximum(
-            jnp.max(s1, axis=1, keepdims=True), jnp.max(s2, axis=1, keepdims=True)
-        )
-        e1 = jnp.exp(s1 - top)
-        e2 = jnp.exp(s2 - top)
-        inv = 1.0 / (jnp.sum(e1, axis=1, keepdims=True) + jnp.sum(e2, axis=1, keepdims=True))
-        o = jnp.dot((e1 * inv).astype(BF16), v_all[at, :], preferred_element_type=F32)
-        o = o + jnp.dot((e2 * inv).astype(BF16), all_cv, preferred_element_type=F32)
-        picked = o[:GRID_W] * masks[0]
-        for h in range(1, half_heads):
-            picked = picked + o[h * GRID_W : (h + 1) * GRID_W] * masks[h]
-        return picked.astype(BF16)
-
-    for i in range(l_rows):
-        att_slab[i * GRID_W : (i + 1) * GRID_W, :] = attend((1 - side) * l_rows + i)
-    back = remote(
-        att_slab, att.at[me_t, side], pair_send.at[3], pair_recv.at[3], mate, me_t
-    )
-    back.start()
-    sends.append(back)
-    wo_forward(1)
-    for i in range(l_rows):
-        att[me_t, side, i * GRID_W : (i + 1) * GRID_W, :] = attend(side * l_rows + i)
-
-    back_in = remote(
-        att_slab, att.at[me_t, 1 - side], pair_send.at[3], pair_recv.at[3], mate, me_t
-    )
-    first, second = att_view(side), att_view(1 - side)
-    gather_start(first, att_sems(0))
-    back_in.wait_recv()
-    gather_start(second, att_sems(1))
-    for c in range(2, n_pieces):
+        s = s + jnp.concatenate([table[first + 2 * m] for m in range(WIN_ROWS // 2)], axis=1)
+        scores[i % 2] = s
+        return at, jnp.max(s, axis=1, keepdims=True)
+
+    def weigh_local(i, at, top):
+        e = jnp.exp(scores[i % 2] - top)
+        tops[i] = jnp.broadcast_to(top, (stack, 128))
+        values_at = jnp.concatenate([v_all[at, :], ones], axis=1)
+        sums[i] = jnp.dot(e.astype(BF16), values_at, preferred_element_type=F32)
+
+    held = score_local(0)
+    for i in range(n_local):
+        later = score_local(i + 1) if i + 1 < n_local else None
+        weigh_local(i, *held)
+        held = later
+
+    for c in range(2, n_pieces - 2):
+        wo_forward(c)
+    for index, block_ctx in enumerate((ctx_k, ctx_v)):
+        for s in range(n_sp):
+            @pl.when((s != me_s) & (s != mate))
+            def _():
+                ctx_copy(index, 0, block_ctx.at[s], s, block_ctx, s).wait_recv()
+
+    all_ck = ctx_k[...].reshape(n_sp * c_rows, half)
+    all_cv = ctx_v[...].reshape(n_sp * c_rows, half)
+    values_ctx = jnp.concatenate([all_cv, jnp.ones((n_sp * c_rows, 128), BF16)], axis=1)
+    top_head = lax.broadcasted_iota(jnp.int32, (GRID_W, half), 1) // HEAD_DIM
+
+    n_ctx = n_sp * c_rows
+    half_stack = l_rows * stack
+
+    def attend_half(which, store):
+        blocks_of = [which * l_rows + i for i in range(l_rows)]
+        qs = q_heads[pl.ds(which * l_rows, l_rows)].reshape(half_stack, half)
+        scores_ctx[...] = lax.dot_general(
+            qs, all_ck, contract_last, preferred_element_type=F32
+        )
+        fades = []
+        for i in range(l_rows):
+            at = slice(i * stack, (i + 1) * stack)
+            s = scores_ctx[at, :]
+            old = tops[blocks_of[i]]
+            top = jnp.maximum(old, jnp.max(s, axis=1, keepdims=True))
+            fades.append(jnp.exp(old - top))
+            wide_top = jnp.concatenate([top] * (n_ctx // 128), axis=1)
+            weights[at, :] = jnp.exp(s - wide_top).astype(BF16)
+        sums_ctx[...] = jnp.dot(weights[...], values_ctx, preferred_element_type=F32)
+        for i in range(l_rows):
+            at = slice(i * stack, (i + 1) * stack)
+            fade = jnp.concatenate([fades[i]] * ((half + 128) // 128), axis=1)
+            o = sums_ctx[at, :] + sums[blocks_of[i]] * fade
+            up, down = o[:, :half], o[:, half:]
+            num, den = up[:GRID_W], down[:GRID_W]
+            for h in range(1, half_heads):
+                part_h = slice(h * GRID_W, (h + 1) * GRID_W)
+                num = jnp.where(top_head == h, up[part_h], num)
+                den = jnp.where(top_head == h, down[part_h], den)
+            store(i, (num / den).astype(BF16))
+
+    def att_copy(index, source, dest, s, t):
+        return remote(source, dest, att_send.at[index], att_recv.at[index], s, t)
+
+    def store_theirs(i, value):
+        att_slab[i * GRID_W : (i + 1) * GRID_W, :] = value
+
+    def store_mine(i, value):
+        att[me_t, side, i * GRID_W : (i + 1) * GRID_W, :] = value
+
+    attend_half(1 - side, store_theirs)
+    begin(att_copy(0, att_slab, att.at[me_t, side], mate, far))
+    begin(att_copy(1, att_slab, att.at[me_t, side], mate, me_t))
+    attend_half(side, store_mine)
+    begin(att_copy(2, att.at[me_t, side], att.at[me_t, side], me_s, far))
+    begin(att_copy(3, att.at[me_t, side], att.at[me_t, side], me_s, partner))
+
+    def arrived(index, shard, part_of):
+        return att_copy(index, att.at[shard, part_of], att.at[shard, part_of], me_s, partner)
+
+    def pass_on(index, onto, shard, part_of):
+        arrived(index, shard, part_of).wait_recv()
+        begin(arrived(onto, shard, part_of))
+
+    for c in range(n_pieces - 2, n_pieces):
         wo_forward(c)
     for c in range(y_pieces):
         wo_cross(c)
@@ -685,47 +760,34 @@
     copies[8].wait()
     cols = 512
 
-    def project(j, first_group, last_group):
-        heads_of = jnp.concatenate([att[j, 0], att[j, 1]], axis=1)
+    def project(groups, last_pass):
+        heads_of = [jnp.concatenate([att[j, 0], att[j, 1]], axis=1) for j in groups]
         for n in range(d // cols):
             at = slice(n * cols, (n + 1) * cols)
-            term = jnp.dot(heads_of, w_out[j, :, at], preferred_element_type=F32)
-            term = term.astype(BF16).astype(F32)
-            if not first_group:
-                term = acc[:, at] + term
-            if last_group:
+            total = None if not last_pass else acc[:, at]
+            for j, lhs in zip(groups, heads_of):
+                term = jnp.dot(lhs, w_out[j, :, at], preferred_element_type=F32)
+                term = term.astype(BF16).astype(F32)
+                total = term if total is None else total + term
+            if last_pass:
                 base = x_in[c_rows:, at].astype(F32)
-                out[:, at] = (base + gate[:, at] * term).astype(BF16)
+                out[:, at] = (base + gate[:, at] * total).astype(BF16)
             else:
-                acc[:, at] = term
-
-    project(me_t, True, False)
-    gather_forward(first, att_sems(0))
-    gather_forward(second, att_sems(1))
+                acc[:, at] = total
+
+    pass_on(1, 5, me_t, 1 - side)
+    pass_on(0, 4, far, 1 - side)
+    pass_on(2, 6, far, side)
+    project((me_t, far), False)
     remote(
         w_out.at[partner], w_out.at[partner], wo_send.at[4, 0], wo_recv.at[4, 0], me_s, partner
     ).wait_recv()
-
-    def att_wait(view, sems):
-        send, recv = sems
-        remote(
-            view(partner), view(partner), send(0), recv(partner), me_s, partner
-        ).wait_recv()
-
-    def att_wait_far(view, sems):
-        send, recv = sems
-        remote(
-            view(far_partner), view(far_partner), send(n_x + 1), recv(far_partner), me_s, partner
-        ).wait_recv()
-
-    att_wait(first, att_sems(0))
-    att_wait(second, att_sems(1))
-    project(partner, False, False)
-    project(far, False, False)
+    arrived(3, partner, side).wait_recv()
+    arrived(5, partner, 1 - side).wait_recv()
     wo_finish_far()
-    att_wait_far(first, att_sems(0))
-    att_wait_far(second, att_sems(1))
-    project(far_partner, False, True)
+    arrived(4, far_partner, 1 - side).wait_recv()
+    arrived(6, far_partner, side).wait_recv()
+    project((partner, far_partner), True)
 
     for c in sends:
         c.wait_send()
@@ -768,6 +830,8 @@
     half = width // 2
     half_heads = heads // 2
     blocks = block // 128
+    l_rows = rows // GRID_W
+    stack = half_heads * GRID_W
     any_spec = pl.BlockSpec(memory_space=pl.ANY)
     vmem_spec = pl.BlockSpec(memory_space=pltpu.VMEM)
     dma = pltpu.SemaphoreType.DMA
@@ -787,10 +851,12 @@
             pltpu.VMEM((rows + c_rows, d), F32),
             pltpu.VMEM((rows + c_rows, d), BF16),
             pltpu.VMEM((3, shift_weight.shape[0], block), BF16),
-            pltpu.VMEM((3, d, width), BF16),
+            pltpu.VMEM((d, 3 * width), BF16),
             pltpu.VMEM((n_tp, width, d), BF16),
             pltpu.VMEM((n_sp, 4 * blocks, 128), F32),
             pltpu.VMEM((n_tp, 4 * blocks, 128), F32),
+            pltpu.VMEM((rows + c_rows, 2 * width), F32),
+            pltpu.VMEM((rows, width), F32),
             pltpu.VMEM((n_sp, blocks, 128), F32),
             pltpu.VMEM((n_tp, blocks, 128), F32),
             pltpu.VMEM((rows, d), F32),
@@ -807,6 +873,13 @@
             pltpu.VMEM((heads, 2 * WIN_ROWS, 2 * GRID_W), F32),
             pltpu.VMEM((half_heads, 2 * WIN_ROWS, 2 * GRID_W), F32),
             pltpu.VMEM((n_pairs, half_heads * GRID_W, 2 * GRID_W), F32),
+            pltpu.VMEM((2 * l_rows, stack, half), BF16),
+            pltpu.VMEM((2, stack, WIN_ROWS * GRID_W), F32),
+            pltpu.VMEM((2 * l_rows, stack, 128), F32),
+            pltpu.VMEM((2 * l_rows, stack, half + 128), F32),
+            pltpu.VMEM((l_rows * stack, n_sp * c_rows), F32),
+            pltpu.VMEM((l_rows * stack, n_sp * c_rows), BF16),
+            pltpu.VMEM((l_rows * stack, half + 128), F32),
             pltpu.VMEM((rows, half), BF16),
             pltpu.VMEM((n_tp, 2, rows, half), BF16),
             dma((15,)),
@@ -826,8 +899,8 @@
             dma((2, n_sp)),
             dma((5, 8)),
             dma((5, 8)),
-            dma((2, n_tp)),
-            dma((2, n_tp)),
+            dma((7,)),
+            dma((7,)),
         ],
         compiler_params=pltpu.CompilerParams(collective_id=0, has_side_effects=True),
         name="fused_block",
@@ -859,7 +932,7 @@
         and condition.shape[0] // n_sp % 128 == 0
         and condition.shape[0] // n_tp % 256 == 0
         and condition.shape[0] // n_tp <= 1024
-        and width % 256 == 0
+        and width == 2 * LANES
         and n_tp == 4
         and n_sp % 2 == 0
     )

time: 37.6 us -> 33.7 us (0.90)
  Pallas kernels: 36.3 us -> 32.5 us
    pallas_call x1, Pallas kernels: 36.3 us -> 32.5 us  [per_device(): pl.pallas_call(functools.partial(fused_kernel, n_sp, n_tp), out_shape=plt...]
where the time goes in v2:
time: 33.7 us; the launch traced here: 33.5 us
  Pallas kernels  32.5 us (96%)
  local copies, waits for them, and re-layouts  0.97 us (3%)
    pallas_call x1, Pallas kernels, per_device(): pl.pallas_call(functools.partial(fused_kernel, n_sp, n_tp), out_shape=plt...  32.5 us
    unnamed x1, local copies, waits for them, and re-layouts  0.97 us

profile of v2, /device:TPU:1, one launch (start us, length us, event | category | flops | bytes accessed | tf_op | source)
XLA Modules:
  0.0 33.5 jit_solution(17396182104651142249)
XLA Ops:
  0.0 32.5 %fused_block.1 = bf16[256,2048]{1,0:T(8,128)(2,1)S(1)} custom-call(bf16[256,2048]{1,0:T(8,128)(2,1)} %latent.1, bf16[64,2048]{1,0:T(8,128)(2,1)} %context.1, bf16[256,512]{1,0:T(8,128)(2,1)} %shift_w.1, bf16[256,512]{1,0:T(8,128)(2,1)} %scale_w.1, bf16[256,512]{1,0:T(8,128)(2,1)} %gate_w.1, bf16[2048,256]{1,0:T(8,128)(2,1)} %query_w.1, ...), custom_call_target="tpu_custom_call" | custom-call | tf_op jit(solution)/shard_map/fused_block/pallas_call | solution.py:838
  32.6 1.0 %copy.17 = bf16[256,2048]{1,0:T(8,128)(2,1)} copy(bf16[256,2048]{1,0:T(8,128)(2,1)S(1)} %fused_block.1) | data formatting | bytes 2097152

commit v3 on v2

--- a/solution.py
+++ b/solution.py
@@ -250,6 +250,7 @@
     halo_recv,
     ctx_send,
     ctx_recv,
+    end_send,
     wo_send,
     wo_recv,
     att_send,
@@ -283,6 +284,17 @@
             device_id=(s, t), device_id_type=MESH,
         )
 
+    barrier = pltpu.get_barrier_semaphore()
+    for k in range(1, n_sp):
+        pl.semaphore_signal(
+            barrier, inc=1, device_id=(lax.rem(me_s + k, n_sp), me_t), device_id_type=MESH
+        )
+    for k in range(1, n_tp):
+        pl.semaphore_signal(
+            barrier, inc=1, device_id=(me_s, lax.rem(me_t + k, n_tp)), device_id_type=MESH
+        )
+    pl.semaphore_signal(barrier, inc=1, device_id=(mate, far), device_id_type=MESH)
+
     loads = [
         (shift_w, w_mod.at[0]),
         (scale_w, w_mod.at[1]),
@@ -304,17 +316,6 @@
     for i in (9, 10, 0, 1, 2, 11, 12, 13, 14, 3, 4):
         copies[i].start()
 
-    barrier = pltpu.get_barrier_semaphore()
-    for k in range(1, n_sp):
-        pl.semaphore_signal(
-            barrier, inc=1, device_id=(lax.rem(me_s + k, n_sp), me_t), device_id_type=MESH
-        )
-    for k in range(1, n_tp):
-        pl.semaphore_signal(
-            barrier, inc=1, device_id=(me_s, lax.rem(me_t + k, n_tp)), device_id_type=MESH
-        )
-    pl.semaphore_signal(barrier, inc=1, device_id=(mate, far), device_id_type=MESH)
-
     def silu(v):
         return v / (1.0 + jnp.exp(-v))
 
@@ -376,18 +377,27 @@
     for b in range(blocks):
         gate_sp[me_s, b : b + 1, :] = gate_part[:1, b * 128 : (b + 1) * 128]
 
-    piece = width // 8
-    y_pieces = 2
-    direct = width - 2 * y_pieces * piece
-
-    def wo_rows(c, at_side):
-        if c < y_pieces:
-            start = direct + at_side * y_pieces * piece + c * piece
+    piece = width // 16
+    n_cross, n_direct = 3, 4
+    n_pieces = 2 * n_cross + n_direct
+    early = (0, n_cross)
+    later = [c + o for c in range(1, n_cross) for o in (0, n_cross)]
+    later = later + list(range(2 * n_cross, n_pieces))
+    z_side = lax.rem(slab, 2)
+    z_mate = me_s + 2 - 4 * z_side
+
+    def wo_rows(c, away_from):
+        if c < n_cross:
+            start = (side + away_from - 2 * side * away_from) * n_cross * piece + c * piece
+        elif c < 2 * n_cross:
+            start = (
+                2 * n_cross * piece
+                + (z_side + away_from - 2 * z_side * away_from) * n_cross * piece
+                + (c - n_cross) * piece
+            )
         else:
-            start = (c - y_pieces) * piece
+            start = (2 * n_cross + c) * piece
         return pl.ds(pl.multiple_of(start, piece), piece)
-
-    n_pieces = direct // piece + y_pieces
 
     def wo_copy(kind, c, source, shard, rows_at, s, t):
         return remote(
@@ -400,18 +410,18 @@
         sends.append(c)
 
     def wo_far(c):
-        return wo_copy(0, c, out_w, me_t, wo_rows(c, side), me_s, far)
+        return wo_copy(0, c, out_w, me_t, wo_rows(c, 0), me_s, far)
 
     def wo_forward(c):
-        at_rows = wo_rows(c, side)
+        at_rows = wo_rows(c, 0)
         came = w_out.at[far]
         wo_copy(0, c, came, far, at_rows, me_s, far).wait_recv()
         begin(wo_copy(1, c, came, far, at_rows, me_s, partner))
-        if c < y_pieces:
-            begin(wo_copy(2, c, came, far, at_rows, mate, me_t))
+        if c < 2 * n_cross:
+            begin(wo_copy(2, c, came, far, at_rows, mate if c < n_cross else z_mate, me_t))
 
     def wo_cross(c):
-        at_rows = wo_rows(c, 1 - side)
+        at_rows = wo_rows(c, 1)
         came = w_out.at[far]
         wo_copy(2, c, came, far, at_rows, mate, me_t).wait_recv()
         begin(wo_copy(3, c, came, far, at_rows, me_s, partner))
@@ -419,11 +429,11 @@
     def wo_finish_far():
         for c in range(n_pieces):
             wo_copy(
-                1, c, w_out.at[far_partner], far_partner, wo_rows(c, side), me_s, partner
+                1, c, w_out.at[far_partner], far_partner, wo_rows(c, 0), me_s, partner
             ).wait_recv()
-        for c in range(y_pieces):
+        for c in range(2 * n_cross):
             wo_copy(
-                3, c, w_out.at[far_partner], far_partner, wo_rows(c, 1 - side), me_s, partner
+                3, c, w_out.at[far_partner], far_partner, wo_rows(c, 1), me_s, partner
             ).wait_recv()
 
     def wo_partner():
@@ -431,7 +441,8 @@
             out_w, w_out.at[me_t], wo_send.at[4, 0], wo_recv.at[4, 0], me_s, partner
         )
 
-    begin(wo_far(0))
+    for c in early:
+        begin(wo_far(c))
 
     copies[3].wait()
     copies[4].wait()
@@ -468,7 +479,7 @@
 
     mod_tp[me_t] = sum_sp(mod_sp, mod_send, mod_recv)
     share_tp(mod_tp, modt_send, modt_recv)
-    for c in range(1, n_pieces):
+    for c in later:
         begin(wo_far(c))
     share_sp(gate_sp, gate_send, gate_recv)
 
@@ -517,10 +528,10 @@
         copies[i].wait()
     part_kv[...] = hidden_dot(chip, 0, 0, 2 * width)
     part_q[...] = hidden_dot(chip, c_rows, 2 * width, width)
+    for c in early:
+        wo_forward(c)
     wait_mod(far)
     wait_mod(far_partner)
-    modulate_pair(1 - chip)
-
     head_row = lax.broadcasted_iota(jnp.int32, (width, width), 0) // HEAD_DIM
     head_col = lax.broadcasted_iota(jnp.int32, (width, width), 1) // HEAD_DIM
     same_head = (head_row == head_col).astype(BF16)
@@ -562,14 +573,49 @@
             s, me_t,
         )
 
-    def along_z(index, slot, source, shard, block_ctx):
+    at_end = (slab == 0) | (slab == last_slab)
+    sends_when = []
+
+    def along_z(index, slot, source, shard, block_ctx, all_direct=False):
         for k in z_order:
-            peer = 2 * lax.rem(slab + k, n_z) + side
-            begin(ctx_copy(index, slot + k, source, shard, block_ctx, peer))
+            peer = lax.rem(slab + k, n_z)
+            c = ctx_copy(index, slot + k, source, shard, block_ctx, 2 * peer + side)
+            low = (peer == 0) & (slab >= 2)
+            high = (peer == last_slab) & (slab <= last_slab - 2)
+            if all_direct:
+                begin(c)
+                continue
+            direct = jnp.logical_not(low | high)
+            pl.when(direct)(c.start)
+            sends_when.append((direct, c))
+
+    z_pair = lax.div(slab, 2)
+
+    def relay_end(of_side):
+        def body():
+            for j in range(2):
+                shard = 2 * (2 * (1 - z_pair) + j) + of_side
+                for index, block_ctx in enumerate((ctx_k, ctx_v)):
+                    ctx_copy(index, 0, block_ctx.at[shard], shard, block_ctx, shard).wait_recv()
+                    end_copy(index, shard, block_ctx).start()
+
+        pl.when(jnp.logical_not(at_end))(body)
+        for j in range(2):
+            shard = 2 * (2 * (1 - z_pair) + j) + of_side
+            for index, block_ctx in enumerate((ctx_k, ctx_v)):
+                sends_when.append((jnp.logical_not(at_end), end_copy(index, shard, block_ctx)))
+
+    def end_copy(index, shard, block_ctx):
+        return remote(
+            block_ctx.at[shard], block_ctx.at[shard],
+            end_send.at[index, shard], ctx_recv.at[index, shard],
+            2 * z_pair * last_slab + side, me_t,
+        )
+
 
     def relay_ctx(index, block_ctx):
         ctx_copy(index, 0, block_ctx.at[mate], mate, block_ctx, mate).wait_recv()
-        along_z(index, n_z - 1, block_ctx.at[mate], mate, block_ctx)
+        along_z(index, n_z - 1, block_ctx.at[mate], mate, block_ctx, True)
 
     lower = rows - GRID_W
 
@@ -596,27 +642,32 @@
         def _():
             up.start()
 
-    both = part_kv[...] + hidden_dot(1 - chip, 0, 0, 2 * width)
+    away = 1 - chip
+    modulate_rows(away, 0, c_rows, vec(away, 1), 1.0 + vec(away, 3))
+    ctx_both = part_kv[:c_rows, :] + jnp.dot(
+        hid[:c_rows, cols_of(away)], w_qkv[cols_of(away), : 2 * width], preferred_element_type=F32
+    )
+    ctx_keys = head_scale(ctx_both[:, :width], key_gain_v)
+    ctx_values = ctx_both[:, width:].astype(BF16)
+    split(ck_stage, ctx_keys)
+    split(cv_stage, ctx_values)
+    for index, (stage, block_ctx) in enumerate(((ck_stage, ctx_k), (cv_stage, ctx_v))):
+        begin(ctx_copy(index, 0, stage.at[1 - side], me_s, block_ctx, mate))
+        along_z(index, 0, stage.at[side], me_s, block_ctx)
+        block_ctx[me_s] = stage[side]
+    modulate_rows(away, c_rows, rows, vec(away, 0), 1.0 + vec(away, 2))
+    both = part_kv[c_rows:, :] + hidden_dot(away, c_rows, 0, 2 * width)
     keys = head_scale(both[:, :width], key_gain_v)
-    split(ck_stage, keys[:c_rows])
-    split(k_stage, keys[c_rows:])
-    begin(ctx_copy(0, 0, ck_stage.at[1 - side], me_s, ctx_k, mate))
+    split(k_stage, keys)
     k_trade = trade(0, k_stage, k_all, own)
     k_all[own, :] = k_stage[side]
     halo_start(True, 0, k_all)
-    along_z(0, 0, ck_stage.at[side], me_s, ctx_k)
-    ctx_k[me_s] = ck_stage[side]
-    values = both[:, width:].astype(BF16)
-    split(cv_stage, values[:c_rows])
-    split(v_stage, values[c_rows:])
-    begin(ctx_copy(1, 0, cv_stage.at[1 - side], me_s, ctx_v, mate))
+    split(v_stage, both[:, width:].astype(BF16))
     v_trade = trade(1, v_stage, v_all, own)
     v_all[own, :] = v_stage[side]
     halo_start(True, 1, v_all)
-    along_z(1, 0, cv_stage.at[side], me_s, ctx_v)
-    ctx_v[me_s] = cv_stage[side]
     queries = head_scale(
-        part_q[...] + hidden_dot(1 - chip, c_rows, 2 * width, width), query_gain_v
+        part_q[...] + hidden_dot(away, c_rows, 2 * width, width), query_gain_v
     ) * jnp.asarray(HEAD_DIM ** (-0.5), BF16)
     split(q_stage, queries)
     q_own = pl.ds(pl.multiple_of(side * rows, rows), rows)
@@ -627,32 +678,34 @@
     share_tp(gate_tp, gatet_send, gatet_recv)
     relay_ctx(0, ctx_k)
     relay_ctx(1, ctx_v)
-    for c in range(y_pieces):
-        wo_forward(c)
+    relay_end(side)
     k_trade.wait_recv()
     halo_start(False, 0, k_all)
+    for c in range(1, n_cross):
+        wo_forward(c)
     v_trade.wait_recv()
     halo_start(False, 1, v_all)
     q_trade.wait_recv()
-    for index, block_all in enumerate((k_all, v_all)):
-        down, up = halo_copies(index, block_all)
-
-        @pl.when(slab < last_slab)
-        def _():
-            down.wait_recv()
-
-        @pl.when(slab > 0)
-        def _():
-            up.wait_recv()
+    def halo_wait(theirs_need):
+        below = side == 0 if theirs_need else side == 1
+        for index, block_all in enumerate((k_all, v_all)):
+            down, up = halo_copies(index, block_all)
+
+            @pl.when(below & (slab < last_slab))
+            def _():
+                down.wait_recv()
+
+            @pl.when(jnp.logical_not(below) & (slab > 0))
+            def _():
+                up.wait_recv()
 
     lane_head = lax.broadcasted_iota(jnp.int32, (GRID_W, half), 1) // HEAD_DIM
     masks = [(lane_head == h).astype(F32) for h in range(half_heads)]
     contract_last = (((1,), (1,)), ((), ()))
     stack = half_heads * GRID_W
-    n_local = 2 * l_rows
     ones = jnp.ones((win, 128), BF16)
 
-    def score_local(i):
+    def score_local(i, held_at, slot):
         start = jnp.where(
             slab == 0,
             jnp.maximum(i, halo),
@@ -661,63 +714,66 @@
         if last_slab == 0:
             start = jnp.int32(halo)
         at = pl.ds(pl.multiple_of(start * GRID_W, GRID_W), win)
-        qi = q_all[i * GRID_W : (i + 1) * GRID_W, :].astype(F32)
+        qi = q_all[pl.ds(pl.multiple_of(i * GRID_W, GRID_W), GRID_W), :].astype(F32)
         qs = jnp.concatenate([(qi * m).astype(BF16) for m in masks], axis=0)
-        q_heads[i] = qs
+        q_heads[held_at] = qs
         s = lax.dot_general(qs, k_all[at, :], contract_last, preferred_element_type=F32)
         first = start - i + WIN_ROWS - 1 - halo
         s = s + jnp.concatenate([table[first + 2 * m] for m in range(WIN_ROWS // 2)], axis=1)
-        scores[i % 2] = s
+        scores[slot] = s
         return at, jnp.max(s, axis=1, keepdims=True)
 
-    def weigh_local(i, at, top):
-        e = jnp.exp(scores[i % 2] - top)
-        tops[i] = jnp.broadcast_to(top, (stack, 128))
+    def weigh_local(held_at, slot, at, top):
+        e = jnp.exp(scores[slot] - top)
+        tops[held_at] = jnp.broadcast_to(top, (stack, 128))
         values_at = jnp.concatenate([v_all[at, :], ones], axis=1)
-        sums[i] = jnp.dot(e.astype(BF16), values_at, preferred_element_type=F32)
-
-    held = score_local(0)
-    for i in range(n_local):
-        later = score_local(i + 1) if i + 1 < n_local else None
-        weigh_local(i, *held)
-        held = later
-
-    for c in range(2, n_pieces - 2):
-        wo_forward(c)
-    for index, block_ctx in enumerate((ctx_k, ctx_v)):
-        for s in range(n_sp):
-            @pl.when((s != me_s) & (s != mate))
-            def _():
-                ctx_copy(index, 0, block_ctx.at[s], s, block_ctx, s).wait_recv()
-
-    all_ck = ctx_k[...].reshape(n_sp * c_rows, half)
-    all_cv = ctx_v[...].reshape(n_sp * c_rows, half)
-    values_ctx = jnp.concatenate([all_cv, jnp.ones((n_sp * c_rows, 128), BF16)], axis=1)
+        sums[held_at] = jnp.dot(e.astype(BF16), values_at, preferred_element_type=F32)
+
+    def local_half(which, base):
+        first = which * l_rows
+        held = score_local(first, base, 0)
+        for i in range(l_rows):
+            later = None
+            if i + 1 < l_rows:
+                later = score_local(first + i + 1, base + i + 1, (i + 1) % 2)
+            weigh_local(base + i, i % 2, *held)
+            held = later
+
+    def ctx_wait():
+        for index, block_ctx in enumerate((ctx_k, ctx_v)):
+            for s in range(n_sp):
+
+                relayed = jnp.logical_not(at_end) & (z_pair != s // 4) & (side == s % 2)
+
+                @pl.when((s != me_s) & (s != mate) & jnp.logical_not(relayed))
+                def _():
+                    ctx_copy(index, 0, block_ctx.at[s], s, block_ctx, s).wait_recv()
+
     top_head = lax.broadcasted_iota(jnp.int32, (GRID_W, half), 1) // HEAD_DIM
-
+    half_stack = l_rows * stack
     n_ctx = n_sp * c_rows
-    half_stack = l_rows * stack
-
-    def attend_half(which, store):
-        blocks_of = [which * l_rows + i for i in range(l_rows)]
-        qs = q_heads[pl.ds(which * l_rows, l_rows)].reshape(half_stack, half)
+    ctx_ones = jnp.ones((n_ctx, 128), BF16)
+
+    def ctx_half(base, store):
+        qs = q_heads[base : base + l_rows].reshape(half_stack, half)
         scores_ctx[...] = lax.dot_general(
-            qs, all_ck, contract_last, preferred_element_type=F32
+            qs, ctx_k[...].reshape(n_ctx, half), contract_last, preferred_element_type=F32
         )
         fades = []
         for i in range(l_rows):
-            at = slice(i * stack, (i + 1) * stack)
-            s = scores_ctx[at, :]
-            old = tops[blocks_of[i]]
+            at_rows = slice(i * stack, (i + 1) * stack)
+            s = scores_ctx[at_rows, :]
+            old = tops[base + i]
             top = jnp.maximum(old, jnp.max(s, axis=1, keepdims=True))
-            fades.append(jnp.exp(old - top))
+            fade = jnp.exp(old - top)
+            fades.append(jnp.concatenate([fade] * ((half + 128) // 128), axis=1))
             wide_top = jnp.concatenate([top] * (n_ctx // 128), axis=1)
-            weights[at, :] = jnp.exp(s - wide_top).astype(BF16)
+            weights[at_rows, :] = jnp.exp(s - wide_top).astype(BF16)
+        values_ctx = jnp.concatenate([ctx_v[...].reshape(n_ctx, half), ctx_ones], axis=1)
         sums_ctx[...] = jnp.dot(weights[...], values_ctx, preferred_element_type=F32)
         for i in range(l_rows):
-            at = slice(i * stack, (i + 1) * stack)
-            fade = jnp.concatenate([fades[i]] * ((half + 128) // 128), axis=1)
-            o = sums_ctx[at, :] + sums[blocks_of[i]] * fade
+            at_rows = slice(i * stack, (i + 1) * stack)
+            o = sums_ctx[at_rows, :] + sums[base + i] * fades[i]
             up, down = o[:, :half], o[:, half:]
             num, den = up[:GRID_W], down[:GRID_W]
             for h in range(1, half_heads):
@@ -735,10 +791,22 @@
     def store_mine(i, value):
         att[me_t, side, i * GRID_W : (i + 1) * GRID_W, :] = value
 
-    attend_half(1 - side, store_theirs)
+    def local_mine():
+        halo_wait(False)
+        local_half(side, l_rows)
+
+    for c in range(n_cross + 1, 2 * n_cross):
+        wo_forward(c)
+    halo_wait(True)
+    local_half(1 - side, 0)
+    no_halo = ((slab == 0) & (side == 0)) | ((slab == last_slab) & (side == 1))
+    pl.when(no_halo)(local_mine)
+    ctx_wait()
+    ctx_half(0, store_theirs)
     begin(att_copy(0, att_slab, att.at[me_t, side], mate, far))
     begin(att_copy(1, att_slab, att.at[me_t, side], mate, me_t))
-    attend_half(side, store_mine)
+    pl.when(jnp.logical_not(no_halo))(local_mine)
+    ctx_half(l_rows, store_mine)
     begin(att_copy(2, att.at[me_t, side], att.at[me_t, side], me_s, far))
     begin(att_copy(3, att.at[me_t, side], att.at[me_t, side], me_s, partner))
 
@@ -749,9 +817,9 @@
         arrived(index, shard, part_of).wait_recv()
         begin(arrived(onto, shard, part_of))
 
-    for c in range(n_pieces - 2, n_pieces):
+    for c in range(2 * n_cross, n_pieces):
         wo_forward(c)
-    for c in range(y_pieces):
+    for c in range(2 * n_cross):
         wo_cross(c)
     wait_tp(gate_tp, gatet_send, gatet_recv)
     gate = jnp.concatenate(
@@ -791,6 +859,8 @@
 
     for c in sends:
         c.wait_send()
+    for condition, c in sends_when:
+        pl.when(condition)(c.wait_send)
     for index, block_all in enumerate((k_all, v_all)):
         down, up = halo_copies(index, block_all)
 
@@ -897,8 +967,9 @@
             dma((2, 2)),
             dma((2, n_sp)),
             dma((2, n_sp)),
-            dma((5, 8)),
-            dma((5, 8)),
+            dma((2, n_sp)),
+            dma((5, 16)),
+            dma((5, 16)),
             dma((7,)),
             dma((7,)),
         ],
@@ -934,7 +1005,7 @@
         and condition.shape[0] // n_tp <= 1024
         and width == 2 * LANES
         and n_tp == 4
-        and n_sp % 2 == 0
+        and n_sp == 8
     )
 
 

time: 33.7 us -> 32.6 us (0.967)
  Pallas kernels: 32.5 us -> 31.3 us
    pallas_call x1, Pallas kernels: 32.5 us -> 31.3 us  [per_device(): pl.pallas_call(functools.partial(fused_kernel, n_sp, n_tp), out_shape=plt...]
where the time goes in v3:
time: 32.6 us; the launch traced here: 32.3 us
  Pallas kernels  31.3 us (96%)
  local copies, waits for them, and re-layouts  0.97 us (3%)
    pallas_call x1, Pallas kernels, per_device(): pl.pallas_call(functools.partial(fused_kernel, n_sp, n_tp), out_shape=plt...  31.3 us
    unnamed x1, local copies, waits for them, and re-layouts  0.97 us

profile of v3, /device:TPU:1, one launch (start us, length us, event | category | flops | bytes accessed | tf_op | source)
XLA Modules:
  0.0 32.3 jit_solution(7512190589644920506)
XLA Ops:
  0.0 31.3 %fused_block.1 = bf16[256,2048]{1,0:T(8,128)(2,1)S(1)} custom-call(bf16[256,2048]{1,0:T(8,128)(2,1)} %latent.1, bf16[64,2048]{1,0:T(8,128)(2,1)} %context.1, bf16[256,512]{1,0:T(8,128)(2,1)} %shift_w.1, bf16[256,512]{1,0:T(8,128)(2,1)} %scale_w.1, bf16[256,512]{1,0:T(8,128)(2,1)} %gate_w.1, bf16[2048,256]{1,0:T(8,128)(2,1)} %query_w.1, ...), custom_call_target="tpu_custom_call" | custom-call | tf_op jit(solution)/shard_map/fused_block/pallas_call | solution.py:908
  31.3 1.0 %copy.17 = bf16[256,2048]{1,0:T(8,128)(2,1)} copy(bf16[256,2048]{1,0:T(8,128)(2,1)S(1)} %fused_block.1) | data formatting | bytes 2097152

commit v4 on v3

--- a/solution.py
+++ b/solution.py
@@ -685,7 +685,6 @@
         wo_forward(c)
     v_trade.wait_recv()
     halo_start(False, 1, v_all)
-    q_trade.wait_recv()
     def halo_wait(theirs_need):
         below = side == 0 if theirs_need else side == 1
         for index, block_all in enumerate((k_all, v_all)):
@@ -739,13 +738,15 @@
             weigh_local(base + i, i % 2, *held)
             held = later
 
-    def ctx_wait():
+    def ctx_wait(wait_near):
         for index, block_ctx in enumerate((ctx_k, ctx_v)):
             for s in range(n_sp):
 
                 relayed = jnp.logical_not(at_end) & (z_pair != s // 4) & (side == s % 2)
 
-                @pl.when((s != me_s) & (s != mate) & jnp.logical_not(relayed))
+                wanted = (z_pair == s // 4) if wait_near else (z_pair != s // 4)
+
+                @pl.when((s != me_s) & (s != mate) & jnp.logical_not(relayed) & wanted)
                 def _():
                     ctx_copy(index, 0, block_ctx.at[s], s, block_ctx, s).wait_recv()
 
@@ -754,23 +755,46 @@
     n_ctx = n_sp * c_rows
     ctx_ones = jnp.ones((n_ctx, 128), BF16)
 
-    def ctx_half(base, store):
+    n_part = n_ctx // 2
+    shards_part = n_sp // 2
+
+    def ctx_scores(base, first_shard, n_keys, exp_all):
+        shards = pl.ds(first_shard, n_keys // c_rows)
         qs = q_heads[base : base + l_rows].reshape(half_stack, half)
-        scores_ctx[...] = lax.dot_general(
-            qs, ctx_k[...].reshape(n_ctx, half), contract_last, preferred_element_type=F32
+        scores_ctx[:, :n_keys] = lax.dot_general(
+            qs, ctx_k[shards].reshape(n_keys, half), contract_last, preferred_element_type=F32
         )
         fades = []
         for i in range(l_rows):
             at_rows = slice(i * stack, (i + 1) * stack)
-            s = scores_ctx[at_rows, :]
+            s = scores_ctx[at_rows, :n_keys]
             old = tops[base + i]
             top = jnp.maximum(old, jnp.max(s, axis=1, keepdims=True))
             fade = jnp.exp(old - top)
             fades.append(jnp.concatenate([fade] * ((half + 128) // 128), axis=1))
-            wide_top = jnp.concatenate([top] * (n_ctx // 128), axis=1)
-            weights[at_rows, :] = jnp.exp(s - wide_top).astype(BF16)
-        values_ctx = jnp.concatenate([ctx_v[...].reshape(n_ctx, half), ctx_ones], axis=1)
-        sums_ctx[...] = jnp.dot(weights[...], values_ctx, preferred_element_type=F32)
+            if exp_all:
+                tops[base + i] = top
+            wide_top = jnp.concatenate([top] * (n_keys // 128), axis=1)
+            weights[at_rows, :n_keys] = jnp.exp(s - wide_top).astype(BF16)
+        values_ctx = jnp.concatenate(
+            [ctx_v[shards].reshape(n_keys, half), ctx_ones[:n_keys]], axis=1
+        )
+        sums_ctx[...] = jnp.dot(
+            weights[:, :n_keys], values_ctx, preferred_element_type=F32
+        )
+        return fades
+
+    def ctx_near(base):
+        fades = ctx_scores(base, shards_part * z_pair, n_part, True)
+        for i in range(l_rows):
+            at_rows = slice(i * stack, (i + 1) * stack)
+            sums[base + i] = sums_ctx[at_rows, :] + sums[base + i] * fades[i]
+
+    def ctx_last(base, store, everything):
+        if everything:
+            fades = ctx_scores(base, 0, n_ctx, False)
+        else:
+            fades = ctx_scores(base, shards_part * (1 - z_pair), n_part, False)
         for i in range(l_rows):
             at_rows = slice(i * stack, (i + 1) * stack)
             o = sums_ctx[at_rows, :] + sums[base + i] * fades[i]
@@ -795,18 +819,33 @@
         halo_wait(False)
         local_half(side, l_rows)
 
+    n_early = len(sends)
     for c in range(n_cross + 1, 2 * n_cross):
         wo_forward(c)
+    no_halo = ((slab == 0) & (side == 0)) | ((slab == last_slab) & (side == 1))
+    pl.when(no_halo)(local_mine)
+    q_trade.wait_recv()
     halo_wait(True)
     local_half(1 - side, 0)
-    no_halo = ((slab == 0) & (side == 0)) | ((slab == last_slab) & (side == 1))
-    pl.when(no_halo)(local_mine)
-    ctx_wait()
-    ctx_half(0, store_theirs)
+    ctx_wait(True)
+    ctx_near(0)
+    @pl.when(no_halo)
+    def _():
+        ctx_near(l_rows)
+
+    ctx_wait(False)
+    ctx_last(0, store_theirs, False)
     begin(att_copy(0, att_slab, att.at[me_t, side], mate, far))
     begin(att_copy(1, att_slab, att.at[me_t, side], mate, me_t))
-    pl.when(jnp.logical_not(no_halo))(local_mine)
-    ctx_half(l_rows, store_mine)
+    @pl.when(no_halo)
+    def _():
+        ctx_last(l_rows, store_mine, False)
+
+    @pl.when(jnp.logical_not(no_halo))
+    def _():
+        local_mine()
+        ctx_last(l_rows, store_mine, True)
+
     begin(att_copy(2, att.at[me_t, side], att.at[me_t, side], me_s, far))
     begin(att_copy(3, att.at[me_t, side], att.at[me_t, side], me_s, partner))
 
@@ -828,11 +867,11 @@
     copies[8].wait()
     cols = 512
 
-    def project(groups, last_pass):
+    def project(groups, first_pass, last_pass):
         heads_of = [jnp.concatenate([att[j, 0], att[j, 1]], axis=1) for j in groups]
         for n in range(d // cols):
             at = slice(n * cols, (n + 1) * cols)
-            total = None if not last_pass else acc[:, at]
+            total = None if first_pass else acc[:, at]
             for j, lhs in zip(groups, heads_of):
                 term = jnp.dot(lhs, w_out[j, :, at], preferred_element_type=F32)
                 term = term.astype(BF16).astype(F32)
@@ -843,34 +882,38 @@
             else:
                 acc[:, at] = total
 
+    for c in sends[:n_early]:
+        c.wait_send()
+    for condition, c in sends_when:
+        pl.when(condition)(c.wait_send)
+    for index, block_all in enumerate((k_all, v_all)):
+        down, up = halo_copies(index, block_all)
+
+        @pl.when(slab > 0)
+        def _():
+            down.wait_send()
+
+        @pl.when(slab < last_slab)
+        def _():
+            up.wait_send()
     pass_on(1, 5, me_t, 1 - side)
+    project((me_t,), True, False)
     pass_on(0, 4, far, 1 - side)
     pass_on(2, 6, far, side)
-    project((me_t, far), False)
+    project((far,), False, False)
     remote(
         w_out.at[partner], w_out.at[partner], wo_send.at[4, 0], wo_recv.at[4, 0], me_s, partner
     ).wait_recv()
     arrived(3, partner, side).wait_recv()
     arrived(5, partner, 1 - side).wait_recv()
+    project((partner,), False, False)
     wo_finish_far()
     arrived(4, far_partner, 1 - side).wait_recv()
     arrived(6, far_partner, side).wait_recv()
-    project((partner, far_partner), True)
-
-    for c in sends:
+    project((far_partner,), False, True)
+
+    for c in sends[n_early:]:
         c.wait_send()
-    for condition, c in sends_when:
-        pl.when(condition)(c.wait_send)
-    for index, block_all in enumerate((k_all, v_all)):
-        down, up = halo_copies(index, block_all)
-
-        @pl.when(slab > 0)
-        def _():
-            down.wait_send()
-
-        @pl.when(slab < last_slab)
-        def _():
-            up.wait_send()
 
 
 def per_device(

time: 32.6 us -> 32.2 us (0.988)
  Pallas kernels: 31.3 us -> 30.8 us
    pallas_call x1, Pallas kernels: 31.3 us -> 30.8 us  [per_device(): pl.pallas_call(functools.partial(fused_kernel, n_sp, n_tp), out_shape=plt...]
where the time goes in v4:
time: 32.2 us; the launch traced here: 31.8 us
  Pallas kernels  30.8 us (96%)
  local copies, waits for them, and re-layouts  0.97 us (3%)
    pallas_call x1, Pallas kernels, per_device(): pl.pallas_call(functools.partial(fused_kernel, n_sp, n_tp), out_shape=plt...  30.8 us
    unnamed x1, local copies, waits for them, and re-layouts  0.97 us

profile of v4, /device:TPU:1, one launch (start us, length us, event | category | flops | bytes accessed | tf_op | source)
XLA Modules:
  0.0 31.8 jit_solution(12012579733907724425)
XLA Ops:
  0.0 30.8 %fused_block.1 = bf16[256,2048]{1,0:T(8,128)(2,1)S(1)} custom-call(bf16[256,2048]{1,0:T(8,128)(2,1)} %latent.1, bf16[64,2048]{1,0:T(8,128)(2,1)} %context.1, bf16[256,512]{1,0:T(8,128)(2,1)} %shift_w.1, bf16[256,512]{1,0:T(8,128)(2,1)} %scale_w.1, bf16[256,512]{1,0:T(8,128)(2,1)} %gate_w.1, bf16[2048,256]{1,0:T(8,128)(2,1)} %query_w.1, ...), custom_call_target="tpu_custom_call" | custom-call | tf_op jit(solution)/shard_map/fused_block/pallas_call | solution.py:951
  30.8 1.0 %copy.17 = bf16[256,2048]{1,0:T(8,128)(2,1)} copy(bf16[256,2048]{1,0:T(8,128)(2,1)S(1)} %fused_block.1) | data formatting | bytes 2097152

commit v5 on v4

--- a/solution.py
+++ b/solution.py
@@ -704,6 +704,10 @@
     stack = half_heads * GRID_W
     ones = jnp.ones((win, 128), BF16)
 
+    def stacked(i):
+        qi = q_all[pl.ds(pl.multiple_of(i * GRID_W, GRID_W), GRID_W), :].astype(F32)
+        return jnp.concatenate([(qi * m).astype(BF16) for m in masks], axis=0)
+
     def score_local(i, held_at, slot):
         start = jnp.where(
             slab == 0,
@@ -713,8 +717,7 @@
         if last_slab == 0:
             start = jnp.int32(halo)
         at = pl.ds(pl.multiple_of(start * GRID_W, GRID_W), win)
-        qi = q_all[pl.ds(pl.multiple_of(i * GRID_W, GRID_W), GRID_W), :].astype(F32)
-        qs = jnp.concatenate([(qi * m).astype(BF16) for m in masks], axis=0)
+        qs = stacked(i)
         q_heads[held_at] = qs
         s = lax.dot_general(qs, k_all[at, :], contract_last, preferred_element_type=F32)
         first = start - i + WIN_ROWS - 1 - halo
@@ -790,21 +793,21 @@
             at_rows = slice(i * stack, (i + 1) * stack)
             sums[base + i] = sums_ctx[at_rows, :] + sums[base + i] * fades[i]
 
-    def ctx_last(base, store, everything):
-        if everything:
-            fades = ctx_scores(base, 0, n_ctx, False)
-        else:
-            fades = ctx_scores(base, shards_part * (1 - z_pair), n_part, False)
+    def finished(o):
+        up, down = o[:, :half], o[:, half:]
+        num, den = up[:GRID_W], down[:GRID_W]
+        for h in range(1, half_heads):
+            part_h = slice(h * GRID_W, (h + 1) * GRID_W)
+            num = jnp.where(top_head == h, up[part_h], num)
+            den = jnp.where(top_head == h, down[part_h], den)
+        return (num / den).astype(BF16)
+
+    def ctx_last(base, store):
+        fades = ctx_scores(base, shards_part * (1 - z_pair), n_part, False)
         for i in range(l_rows):
             at_rows = slice(i * stack, (i + 1) * stack)
             o = sums_ctx[at_rows, :] + sums[base + i] * fades[i]
-            up, down = o[:, :half], o[:, half:]
-            num, den = up[:GRID_W], down[:GRID_W]
-            for h in range(1, half_heads):
-                part_h = slice(h * GRID_W, (h + 1) * GRID_W)
-                num = jnp.where(top_head == h, up[part_h], num)
-                den = jnp.where(top_head == h, down[part_h], den)
-            store(i, (num / den).astype(BF16))
+            store(i, finished(o))
 
     def att_copy(index, source, dest, s, t):
         return remote(source, dest, att_send.at[index], att_recv.at[index], s, t)
@@ -814,6 +817,43 @@
 
     def store_mine(i, value):
         att[me_t, side, i * GRID_W : (i + 1) * GRID_W, :] = value
+
+    def ctx_start():
+        for i in range(l_rows):
+            q_heads[l_rows + i] = stacked(side * l_rows + i)
+        qs = q_heads[l_rows : 2 * l_rows].reshape(half_stack, half)
+        scores_ctx[...] = lax.dot_general(
+            qs, ctx_k[...].reshape(n_ctx, half), contract_last, preferred_element_type=F32
+        )
+        for i in range(l_rows):
+            at_rows = slice(i * stack, (i + 1) * stack)
+            s = scores_ctx[at_rows, :]
+            top = jnp.broadcast_to(jnp.max(s, axis=1, keepdims=True), (stack, 128))
+            tops[l_rows + i] = top
+            wide_top = jnp.concatenate([top] * (n_ctx // 128), axis=1)
+            weights[at_rows, :] = jnp.exp(s - wide_top).astype(BF16)
+        values_ctx = jnp.concatenate([ctx_v[...].reshape(n_ctx, half), ctx_ones], axis=1)
+        sums_ctx[...] = jnp.dot(weights[...], values_ctx, preferred_element_type=F32)
+
+    def local_last():
+        first = side * l_rows
+        held = score_local(first, l_rows, 0)
+        for i in range(l_rows):
+            later = None
+            if i + 1 < l_rows:
+                later = score_local(first + i + 1, l_rows + i + 1, (i + 1) % 2)
+            at, top = held
+            at_rows = slice(i * stack, (i + 1) * stack)
+            old = tops[l_rows + i]
+            top = jnp.maximum(old, top)
+            wide_top = jnp.concatenate([top] * (win // 128), axis=1)
+            e = jnp.exp(scores[i % 2] - wide_top)
+            values_at = jnp.concatenate([v_all[at, :], ones], axis=1)
+            o = jnp.dot(e.astype(BF16), values_at, preferred_element_type=F32)
+            fade = jnp.exp(old - top)
+            o = o + sums_ctx[at_rows, :] * jnp.concatenate([fade] * ((half + 128) // 128), axis=1)
+            store_mine(i, finished(o))
+            held = later
 
     def local_mine():
         halo_wait(False)
@@ -823,28 +863,33 @@
     for c in range(n_cross + 1, 2 * n_cross):
         wo_forward(c)
     no_halo = ((slab == 0) & (side == 0)) | ((slab == last_slab) & (side == 1))
-    pl.when(no_halo)(local_mine)
+    @pl.when(no_halo)
+    def _():
+        local_mine()
+        ctx_wait(True)
+        ctx_near(l_rows)
+
     q_trade.wait_recv()
     halo_wait(True)
     local_half(1 - side, 0)
-    ctx_wait(True)
+    @pl.when(jnp.logical_not(no_halo))
+    def _():
+        ctx_wait(True)
+
     ctx_near(0)
-    @pl.when(no_halo)
-    def _():
-        ctx_near(l_rows)
-
     ctx_wait(False)
-    ctx_last(0, store_theirs, False)
+    ctx_last(0, store_theirs)
     begin(att_copy(0, att_slab, att.at[me_t, side], mate, far))
     begin(att_copy(1, att_slab, att.at[me_t, side], mate, me_t))
     @pl.when(no_halo)
     def _():
-        ctx_last(l_rows, store_mine, False)
+        ctx_last(l_rows, store_mine)
 
     @pl.when(jnp.logical_not(no_halo))
     def _():
-        local_mine()
-        ctx_last(l_rows, store_mine, True)
+        ctx_start()
+        halo_wait(False)
+        local_last()
 
     begin(att_copy(2, att.at[me_t, side], att.at[me_t, side], me_s, far))
     begin(att_copy(3, att.at[me_t, side], att.at[me_t, side], me_s, partner))
@@ -897,20 +942,33 @@
         def _():
             up.wait_send()
     pass_on(1, 5, me_t, 1 - side)
+    pass_on(0, 4, far, 1 - side)
     project((me_t,), True, False)
-    pass_on(0, 4, far, 1 - side)
     pass_on(2, 6, far, side)
-    project((far,), False, False)
+    odd = core == 1
+    @pl.when(odd)
+    def _():
+        project((far,), False, False)
+
     remote(
         w_out.at[partner], w_out.at[partner], wo_send.at[4, 0], wo_recv.at[4, 0], me_s, partner
     ).wait_recv()
     arrived(3, partner, side).wait_recv()
     arrived(5, partner, 1 - side).wait_recv()
-    project((partner,), False, False)
+    @pl.when(odd)
+    def _():
+        project((partner,), False, False)
+
     wo_finish_far()
     arrived(4, far_partner, 1 - side).wait_recv()
     arrived(6, far_partner, side).wait_recv()
-    project((far_partner,), False, True)
+    @pl.when(odd)
+    def _():
+        project((far_partner,), False, True)
+
+    @pl.when(jnp.logical_not(odd))
+    def _():
+        project((far, partner, far_partner), False, True)
 
     for c in sends[n_early:]:
         c.wait_send()

time: 32.2 us -> 31.8 us (0.988)
  no operation moved by 1% of the time
where the time goes in v5:
time: 31.8 us; the launch traced here: 31.6 us
  Pallas kernels  30.6 us (96%)
  local copies, waits for them, and re-layouts  0.97 us (3%)
    pallas_call x1, Pallas kernels, per_device(): pl.pallas_call(functools.partial(fused_kernel, n_sp, n_tp), out_shape=plt...  30.6 us
    unnamed x1, local copies, waits for them, and re-layouts  0.97 us

profile of v5, /device:TPU:1, one launch (start us, length us, event | category | flops | bytes accessed | tf_op | source)
XLA Modules:
  0.0 31.6 jit_solution(9823785893345624666)
XLA Ops:
  0.0 30.6 %fused_block.1 = bf16[256,2048]{1,0:T(8,128)(2,1)S(1)} custom-call(bf16[256,2048]{1,0:T(8,128)(2,1)} %latent.1, bf16[64,2048]{1,0:T(8,128)(2,1)} %context.1, bf16[256,512]{1,0:T(8,128)(2,1)} %shift_w.1, bf16[256,512]{1,0:T(8,128)(2,1)} %scale_w.1, bf16[256,512]{1,0:T(8,128)(2,1)} %gate_w.1, bf16[2048,256]{1,0:T(8,128)(2,1)} %query_w.1, ...), custom_call_target="tpu_custom_call" | custom-call | tf_op jit(solution)/shard_map/fused_block/pallas_call | solution.py:1009
  30.6 1.0 %copy.17 = bf16[256,2048]{1,0:T(8,128)(2,1)} copy(bf16[256,2048]{1,0:T(8,128)(2,1)S(1)} %fused_block.1) | data formatting | bytes 2097152

commit v6 on v5

--- a/solution.py
+++ b/solution.py
@@ -343,7 +343,8 @@
 
     def share_sp(buf, send, recv):
         for k in range(1, n_sp):
-            peer = lax.rem(me_s + k, n_sp)
+            away_first = jnp.where(slab <= last_slab // 2, n_sp - k, k)
+            peer = lax.rem(me_s + away_first, n_sp)
             c = remote(buf.at[me_s], buf.at[me_s], send.at[k], recv.at[me_s], peer, me_t)
             c.start()
             sends.append(c)

time: 31.8 us -> 31.8 us (level)
  no operation moved by 1% of the time
where the time goes in v6:
time: 31.8 us; the launch traced here: 31.6 us
  Pallas kernels  30.6 us (96%)
  local copies, waits for them, and re-layouts  0.97 us (3%)
    pallas_call x1, Pallas kernels, per_device(): pl.pallas_call(functools.partial(fused_kernel, n_sp, n_tp), out_shape=plt...  30.6 us
    unnamed x1, local copies, waits for them, and re-layouts  0.97 us

profile of v6, /device:TPU:1, one launch (start us, length us, event | category | flops | bytes accessed | tf_op | source)
XLA Modules:
  0.0 31.6 jit_solution(17460895470153579882)
XLA Ops:
  0.0 30.6 %fused_block.1 = bf16[256,2048]{1,0:T(8,128)(2,1)S(1)} custom-call(bf16[256,2048]{1,0:T(8,128)(2,1)} %latent.1, bf16[64,2048]{1,0:T(8,128)(2,1)} %context.1, bf16[256,512]{1,0:T(8,128)(2,1)} %shift_w.1, bf16[256,512]{1,0:T(8,128)(2,1)} %scale_w.1, bf16[256,512]{1,0:T(8,128)(2,1)} %gate_w.1, bf16[2048,256]{1,0:T(8,128)(2,1)} %query_w.1, ...), custom_call_target="tpu_custom_call" | custom-call | tf_op jit(solution)/shard_map/fused_block/pallas_call | solution.py:1010
  30.6 1.0 %copy.17 = bf16[256,2048]{1,0:T(8,128)(2,1)} copy(bf16[256,2048]{1,0:T(8,128)(2,1)S(1)} %fused_block.1) | data formatting | bytes 2097152
